TPU v7x, 32 devices: a whole 2x2x4 slice. The times are simulated.
32 devices in a mesh: kv: 8 (over z, y), tp: 4 (over x, core).
Axes of the slice: x: 2, y: 2, z: 4, core: 2. Of those that a mesh axis runs over, the one named last changes fastest.
Arguments:
- queries: bfloat16 [6144, 2048], P('kv', 'tp'), may hold values from -6 to 6
- keys_values: bfloat16 [6144, 1024], P('kv', 'tp'), may hold values from -6 to 6
- log_sums: float32 [6144, 32], P('kv', 'tp'), may hold values from 6.5 to 7.5
- out_grad: bfloat16 [6144, 2048], P('kv', 'tp'), may hold values from -96 to 96
- inputs: bfloat16 [6144, 4096], P('kv'), may hold values from -0.046875 to 0.046875
- chosen: int32 [48, 16], P('kv'), may hold values from -1 to 95, as said below
Outputs:
- query_grad: bfloat16 [6144, 2048], P('kv', 'tp')
- kv_grad: float32 [6144, 1024], P('kv', 'tp')
- weight_grad: float32 [4096, 2048], P('kv', 'tp')
Inputs may be any that keep to these rules, and one draw needn't show every extreme that they name: `chosen`: each row names distinct key blocks, none starting after the last position of that row's query block, and -1 in unused entries; at least half of 16 blocks are named where that many are allowed. From the query blocks of one index of kv, at most 6 distinct blocks of the 768 positions of any one index are named, and this most is reached on every index.
All inputs are finite; a program needn't handle non-finite values.
Results may differ from a plain program's by a relative error of at most 0.0051.
Values may be sent and summed in bfloat16 or wider, within the bound.
A program may use at most 128 MiB of HBM per device.

v0:
```python
import functools

import jax
import jax.numpy as jnp
from jax import lax
from jax.experimental import pallas as pl
from jax.experimental.pallas import tpu as pltpu
from jax.sharding import PartitionSpec as P

DH = 64
BLK = 64
QB = 128
NSEL = 16
CHUNK = 4
SCALE = DH ** (-0.5)


def attend(group_size, slot_ref, chosen_ref, base_ref, tab_ref, w1_ref, w2_ref, ls_ref, dq_ref, g_ref,
           kv_scr, p_scr, dp_scr, a_scr):
    qb = pl.program_id(1)
    lanes = group_size * QB
    rows = CHUNK * BLK

    @pl.when(qb == 0)
    def _():
        g_ref[...] = jnp.zeros_like(g_ref)

    starts = [pl.multiple_of(slot_ref[qb, j] * BLK, BLK) for j in range(NSEL)]
    for j in range(NSEL):
        kv_scr[j * BLK:(j + 1) * BLK, :] = tab_ref[pl.ds(starts[j], BLK), :]
    lane = lax.broadcasted_iota(jnp.int32, (1, lanes), 1)
    qpos = (base_ref[0] + qb) * QB + lax.rem(lane, QB)
    within = lax.broadcasted_iota(jnp.int32, (BLK, lanes), 0)
    sums = ls_ref[0, 0]
    delta = jnp.zeros((1, lanes), jnp.float32)
    for c in range(NSEL // CHUNK):
        kv = kv_scr[c * rows:(c + 1) * rows, :]
        scores = jnp.dot(kv, w1_ref[0, 0, :, :lanes], preferred_element_type=jnp.float32)
        grads = jnp.dot(kv, w1_ref[0, 0, :, lanes:], preferred_element_type=jnp.float32)
        for i in range(CHUNK):
            block = chosen_ref[qb, c * CHUNK + i]
            last = jnp.where(block >= 0, qpos - block * BLK, -1)
            here = slice(i * BLK, (i + 1) * BLK)
            there = slice(c * rows + i * BLK, c * rows + (i + 1) * BLK)
            prob = jnp.where(within <= last, jnp.exp(scores[here] - sums), jnp.float32(0.0))
            rounded = prob.astype(jnp.bfloat16)
            delta += jnp.sum(rounded.astype(jnp.float32) * grads[here], axis=0, keepdims=True)
            p_scr[there, :] = prob
            dp_scr[there, :] = grads[here]
            a_scr[there, lanes:] = rounded
    for c in range(NSEL // CHUNK):
        there = slice(c * rows, (c + 1) * rows)
        a_scr[there, :lanes] = (p_scr[there, :] * (dp_scr[there, :] - delta)).astype(jnp.bfloat16)
        both = jnp.dot(a_scr[there, :], w2_ref[0, 0], preferred_element_type=jnp.float32)
        for i in range(CHUNK):
            at = pl.ds(starts[c * CHUNK + i], BLK)
            g_ref[at, :] = g_ref[at, :] + both[i * BLK:(i + 1) * BLK]
    dq_t = jnp.dot(kv_scr[...].T, a_scr[:, :lanes], preferred_element_type=jnp.float32)[:DH] * SCALE
    stacked = jnp.concatenate([dq_t[:, g * QB:(g + 1) * QB] for g in range(group_size)], axis=0)
    dq_ref[...] = stacked.T.astype(jnp.bfloat16)


def gather_sum(target_ref, part_ref, out_ref):
    out_ref[...] = jnp.zeros_like(out_ref)

    def step(i, carry):
        target = target_ref[i]

        @pl.when(target >= 0)
        def _():
            at = pl.ds(pl.multiple_of(target * BLK, BLK), BLK)
            frm = pl.ds(pl.multiple_of(i * BLK, BLK), BLK)
            out_ref[at, :] = out_ref[at, :] + part_ref[frm, :].astype(jnp.float32)

        return carry

    lax.fori_loop(0, target_ref.shape[0], step, 0)


def shards(queries, keys_values, log_sums, out_grad, inputs, chosen):
    tok_count = queries.shape[0]
    heads_here = queries.shape[1] // DH
    kv_heads = keys_values.shape[1] // (2 * DH)
    group_size = heads_here // kv_heads
    row_width = keys_values.shape[1]
    blocks_here = tok_count // BLK
    query_blocks = tok_count // QB
    kv_count = lax.axis_size("kv")
    first_block = lax.axis_index("kv") * query_blocks
    capacity = blocks_here // 2
    total_blocks = kv_count * blocks_here
    lanes = group_size * QB
    flat_ids = chosen.reshape(-1)
    needed = jnp.any(
        flat_ids[:, None] == jnp.arange(total_blocks, dtype=jnp.int32)[None, :], axis=0
    )
    needed = needed.reshape(kv_count, blocks_here).astype(jnp.int32)
    rank_in = jnp.cumsum(needed, axis=1) - 1
    matches = (needed[:, :, None] == 1) & (
        rank_in[:, :, None] == jnp.arange(capacity, dtype=jnp.int32)[None, None, :]
    )
    request = jnp.sum(
        matches.astype(jnp.int32) * jnp.arange(blocks_here, dtype=jnp.int32)[None, :, None], axis=1
    )
    request = jnp.where(jnp.any(matches, axis=1), request, -1)
    slot_flat = (jnp.arange(kv_count, dtype=jnp.int32)[:, None] * capacity + rank_in).reshape(-1)
    one_hot = chosen[:, :, None] == jnp.arange(total_blocks, dtype=jnp.int32)[None, None, :]
    slot_ids = jnp.sum(jnp.where(one_hot, slot_flat[None, None, :], 0), axis=2)
    asked_ids = lax.all_to_all(request, "kv", split_axis=0, concat_axis=0, tiled=True)
    local_blocks = keys_values.reshape(blocks_here, BLK, row_width)
    fetched = local_blocks[jnp.maximum(asked_ids, 0)]
    key_table = lax.all_to_all(fetched, "kv", split_axis=0, concat_axis=0, tiled=True).reshape(
        kv_count * capacity * BLK, row_width
    )

    def heads_first(rows):
        split = rows.reshape(query_blocks, QB, kv_heads, group_size, DH)
        return split.transpose(0, 2, 3, 1, 4).reshape(query_blocks, kv_heads, lanes, DH)

    query_rows = heads_first(queries * jnp.bfloat16(SCALE))
    grad_rows = heads_first(out_grad)
    pad = ((0, 0), (0, 0), (0, 0))
    w2 = jnp.concatenate(
        [jnp.pad(query_rows, pad + ((0, DH),)), jnp.pad(grad_rows, pad + ((DH, 0),))], axis=2
    )
    w1 = w2.swapaxes(2, 3)
    sums = (
        log_sums.reshape(query_blocks, QB, kv_heads, group_size)
        .transpose(0, 2, 3, 1)
        .reshape(query_blocks, kv_heads, 1, lanes)
    )
    table_rows = kv_count * capacity * BLK
    keys = NSEL * BLK
    query_grad, grad_table = pl.pallas_call(
        functools.partial(attend, group_size),
        grid_spec=pltpu.PrefetchScalarGridSpec(
            num_scalar_prefetch=3,
            grid=(kv_heads, query_blocks),
            in_specs=[
                pl.BlockSpec((table_rows, 2 * DH), lambda h, q, *_: (0, h)),
                pl.BlockSpec((1, 1, 2 * DH, 2 * lanes), lambda h, q, *_: (q, h, 0, 0)),
                pl.BlockSpec((1, 1, 2 * lanes, 2 * DH), lambda h, q, *_: (q, h, 0, 0)),
                pl.BlockSpec((1, 1, 1, lanes), lambda h, q, *_: (q, h, 0, 0)),
            ],
            out_specs=[
                pl.BlockSpec((QB, group_size * DH), lambda h, q, *_: (q, h)),
                pl.BlockSpec((table_rows, 2 * DH), lambda h, q, *_: (0, h)),
            ],
            scratch_shapes=[
                pltpu.VMEM((keys, 2 * DH), jnp.bfloat16),
                pltpu.VMEM((keys, lanes), jnp.float32),
                pltpu.VMEM((keys, lanes), jnp.float32),
                pltpu.VMEM((keys, 2 * lanes), jnp.bfloat16),
            ],
        ),
        out_shape=[
            jax.ShapeDtypeStruct((tok_count, heads_here * DH), jnp.bfloat16),
            jax.ShapeDtypeStruct((table_rows, row_width), jnp.float32),
        ],
        compiler_params=pltpu.CompilerParams(
            dimension_semantics=("arbitrary", "arbitrary"), vmem_limit_bytes=48 * 1024 * 1024
        ),
        cost_estimate=pl.CostEstimate(
            flops=12 * query_blocks * QB * keys * heads_here * DH,
            bytes_accessed=16 * 1024 * 1024,
            transcendentals=query_blocks * QB * keys * heads_here,
        ),
    )(slot_ids, chosen, first_block[None].astype(jnp.int32), key_table, w1, w2, sums)
    weight_part = lax.dot_general(
        inputs, query_grad, (((0,), (0,)), ((), ())), preferred_element_type=jnp.float32
    ).astype(jnp.bfloat16)
    weight_grad = lax.psum_scatter(weight_part, "kv", scatter_dimension=0, tiled=True).astype(
        jnp.float32
    )
    returned = lax.all_to_all(
        grad_table.astype(jnp.bfloat16).reshape(kv_count, capacity * BLK, row_width),
        "kv",
        split_axis=0,
        concat_axis=0,
        tiled=True,
    ).reshape(table_rows, row_width)
    kv_grad = pl.pallas_call(
        gather_sum,
        in_specs=[
            pl.BlockSpec(memory_space=pltpu.SMEM),
            pl.BlockSpec(memory_space=pltpu.VMEM),
        ],
        out_specs=pl.BlockSpec(memory_space=pltpu.VMEM),
        out_shape=jax.ShapeDtypeStruct((tok_count, row_width), jnp.float32),
    )(asked_ids.reshape(-1), returned)
    return (query_grad, kv_grad, weight_grad)


def solution(mesh):
    in_specs = (
        P("kv", "tp"),
        P("kv", "tp"),
        P("kv", "tp"),
        P("kv", "tp"),
        P("kv", None),
        P("kv", None),
    )
    out_specs = (P("kv", "tp"), P("kv", "tp"), P("kv", "tp"))
    return jax.shard_map(shards, mesh=mesh, in_specs=in_specs, out_specs=out_specs, check_vma=False)
```

profile of v0, /device:TPU:0, one launch (start us, length us, event | category | flops | bytes accessed | tf_op | source)
XLA Modules:
  0.0 235.9 jit_solution(426219408771217337)
XLA Ops:
  7.2 0.0 copy-start
  7.2 0.8 eq.55
  8.0 0.1 fusion.4
  8.1 0.1 reshape.113
  8.2 0.2 reduce_window_sum.11
  8.4 0.1 broadcast_add_fusion
  8.4 0.2 fusion.6
  8.6 0.2 select_reduce_fusion.1
  8.8 0.1 copy.30
  8.9 13.6 %all_to_all.16 = s32[8,1,6]{2,1,0:T(1,128)S(1)} all-to-all(s32[8,1,6]{2,1,0:T(1,128)S(1)} %copy.30), channel_id=1, replica_groups=mesh['kv'=8,'tp'=4] {'kv'}, dimensions={0} | all-to-all | bytes 384 | tf_op jit(solution)/shard_map/all_to_all | solution.py:109
  22.5 0.5 broadcast.88
  23.0 0.7 fusion.8
  23.7 0.1 reshape.116
  23.8 0.0 copy-done
  23.8 0.0 copy-start.7
  23.8 0.0 copy-start.6
  23.8 1.9 gather_fusion
  25.7 3.6 %all-to-all-start.1 = ((bf16[8,6,64,256]{3,2,1,0:T(8,128)(2,1)}), bf16[8,6,64,256]{3,2,1,0:T(8,128)(2,1)S(1)}, u32[]{:S(2)}, u32[]{:S(2)}) async-start(bf16[8,6,64,256]{3,2,1,0:T(8,128)(2,1)} %bitcast.3), calls=%async_computation.1 | async-start | bytes 3145728 | tf_op jit(solution)/shard_map/all_to_all | solution.py:112
  29.3 0.0 reduce-scatter.2.cloned.1.call-start
  29.3 0.1 add.35
  29.4 0.0 copy-done.7
  29.4 0.6 copy.35
  30.0 0.0 copy-done.6
  30.0 0.1 broadcast_multiply_fusion
  30.1 0.3 copy.31
  30.4 1.9 reshape.104
  32.2 2.0 copy.32
  34.2 2.3 copy.33
  36.5 2.7 %reshape.106 = bf16[6,128,2,4,64]{1,0,4,3,2:T(8,128)(2,1)} reshape(bf16[768,512]{0,1:T(8,128)(2,1)} %copy.33) | data formatting | bytes 1572864 | tf_op jit(solution)/shard_map/reshape | solution.py:117
  39.2 2.7 %copy.34 = bf16[6,2,4,128,64]{4,3,2,1,0:T(8,128)(2,1)} copy(bf16[6,2,4,128,64]{3,0,4,2,1:T(8,128)(2,1)} %bitcast.34) | data formatting | bytes 1572864 | tf_op jit(solution)/shard_map/transpose | solution.py:118
  41.9 4.5 %fusion.3 = (bf16[6,2,1024,128]{3,2,1,0:T(8,128)(2,1)}, bf16[6,2,128,1024]{2,3,1,0:T(8,128)(2,1)}) fusion(bf16[6,2,512,64]{3,2,1,0:T(8,128)(2,1)} %bitcast.31, bf16[6,2,512,64]{3,2,1,0:T(8,128)(2,1)S(1)} %bitcast.30), kind=kLoop, calls=%fused_computation.7 | loop fusion | flops 12582912 | bytes 7864320 | tf_op jit(solution)/shard_map/concatenate | solution.py:123
  46.4 4.7 %copy.36.w1_ref = bf16[6,2,128,1024]{3,2,1,0:T(8,128)(2,1)} copy(bf16[6,2,128,1024]{2,3,1,0:T(8,128)(2,1)} %get-tuple-element.22) | data formatting | bytes 6291456 | tf_op jit(solution)/shard_map/transpose | solution.py:126
  51.1 0.2 select_reduce_fusion.slot_ref
  51.3 13.9 %all-to-all-done.1 = bf16[8,6,64,256]{3,2,1,0:T(8,128)(2,1)S(1)} async-done(((bf16[8,6,64,256]{3,2,1,0:T(8,128)(2,1)}), bf16[8,6,64,256]{3,2,1,0:T(8,128)(2,1)S(1)}, u32[]{:S(2)}, u32[]{:S(2)}) %all-to-all-start.1) | async-done | bytes 1572896 | tf_op jit(solution)/shard_map/all_to_all | solution.py:112
  65.2 1.1 copy-done.1
  66.4 1.4 copy-done.2
  67.8 0.7 copy-done.3
  68.5 29.6 %shard_map.85 = (bf16[768,512]{1,0:T(8,128)(2,1)}, f32[3072,256]{1,0:T(8,128)S(1)}) custom-call(s32[6,16]{1,0:T(8,128)S(1)} %select_reduce_fusion.slot_ref, s32[6,16]{1,0:T(8,128)S(1)} %copy-done.4, s32[1]{0:T(128)} %bitcast.base_ref, bf16[3072,256]{1,0:T(8,128)(2,1)S(1)} %bitcast.27, bf16[6,2,128,1024]{3,2,1,0:T(8,128)(2,1)} %copy.36.w1_ref, ...), custom_call_target="tpu_custom_call" | custom-call | flops 4831838208 | bytes 16777216 | tf_op jit(solution)/shard_map/pallas_call | solution.py:134
  98.1 8.4 %fusion.2 = bf16[4096,512]{0,1:T(8,128)(2,1)} fusion(bf16[768,512]{1,0:T(8,128)(2,1)} %get-tuple-element.16, bf16[768,4096]{1,0:T(8,128)(2,1)} %param.10), kind=kOutput, calls=%fused_computation.6 | convolution fusion | flops 3223322624 | bytes 11272192 | tf_op jit(solution)/shard_map/dot_general | solution.py:169
  106.6 0.0 reduce-scatter.2.cloned.1.call-update
  106.6 1.3 convert_element_type.29
  107.9 3.6 %all-to-all-start.2 = ((bf16[8,384,256]{2,1,0:T(8,128)(2,1)}), bf16[8,384,256]{2,1,0:T(8,128)(2,1)S(1)}, u32[]{:S(2)}, u32[]{:S(2)}) async-start(bf16[8,384,256]{2,1,0:T(8,128)(2,1)} %bitcast.32), calls=%async_computation.2 | async-start | bytes 3145728 | tf_op jit(solution)/shard_map/all_to_all | solution.py:175
  111.5 0.6 reshape.110.target_ref
  112.1 70.1 %all-to-all-done.2 = bf16[8,384,256]{2,1,0:T(8,128)(2,1)S(1)} async-done(((bf16[8,384,256]{2,1,0:T(8,128)(2,1)}), bf16[8,384,256]{2,1,0:T(8,128)(2,1)S(1)}, u32[]{:S(2)}, u32[]{:S(2)}) %all-to-all-start.2) | async-done | bytes 1572896 | tf_op jit(solution)/shard_map/all_to_all | solution.py:175
  182.2 1.2 copy-done.5
  183.3 3.1 %shard_map.86 = f32[768,256]{1,0:T(8,128)} custom-call(s32[48]{0:T(128)} %reshape.110.target_ref, bf16[3072,256]{1,0:T(8,128)(2,1)} %bitcast.29), custom_call_target="tpu_custom_call" | custom-call | tf_op jit(solution)/shard_map/pallas_call | solution.py:182
  186.5 40.4 %reduce-scatter.2.cloned.1.call-done = bf16[512,512]{0,1:T(8,128)(2,1)} async-done(((bf16[4096,512]{0,1:T(8,128)(2,1)}), bf16[512,512]{0,1:T(8,128)(2,1)}) %reduce-scatter.2.cloned.1.call-update) | async-done | bytes 524304 | tf_op jit(solution)/shard_map/reduce_scatter | solution.py:172
  226.8 2.2 copy.37
  (12 shorter events, 0.0 us)
Async XLA Ops:
  7.2 16.6 %copy-start = (bf16[768,256]{1,0:T(8,128)(2,1)S(1)}, bf16[768,256]{1,0:T(8,128)(2,1)}, u32[]{:S(2)}) copy-start(bf16[768,256]{1,0:T(8,128)(2,1)} %param.7) | copy-start | bytes 1179652
  23.8 5.6 %copy-start.7 = (f32[768,8]{0,1:T(8,128)S(1)}, f32[768,8]{0,1:T(8,128)}, u32[]{:S(2)}) copy-start(f32[768,8]{0,1:T(8,128)} %param.8) | copy-start | bytes 73732
  23.8 6.2 %copy-start.6 = (bf16[768,512]{1,0:T(8,128)(2,1)S(1)}, bf16[768,512]{1,0:T(8,128)(2,1)}, u32[]{:S(2)}) copy-start(bf16[768,512]{1,0:T(8,128)(2,1)} %param.6) | copy-start | bytes 2359300
  25.7 39.5 %all-to-all-start.1 = ((bf16[8,6,64,256]{3,2,1,0:T(8,128)(2,1)}), bf16[8,6,64,256]{3,2,1,0:T(8,128)(2,1)S(1)}, u32[]{:S(2)}, u32[]{:S(2)}) async-start(bf16[8,6,64,256]{3,2,1,0:T(8,128)(2,1)} %bitcast.3), calls=%async_computation.1 | async-start | bytes 3145728 | tf_op jit(solution)/shard_map/all_to_all | solution.py:112
  29.3 197.6 %reduce-scatter.2.cloned.1.call-start = ((), (), s32[]{:S(2)}) async-start(), calls=%async_computation.4 | async-start | bytes 4718592 | tf_op jit(solution)/shard_map/reduce_scatter | solution.py:172
  46.4 4.7 %copy-start.4 = (s32[6,16]{1,0:T(8,128)S(1)}, s32[6,16]{1,0:T(8,128)}, u32[]{:S(2)}) copy-start(s32[6,16]{1,0:T(8,128)} %chosen_ref.1) | copy-start | bytes 1156
  65.2 1.1 copy-start.1
  66.4 1.4 copy-start.2
  67.8 0.7 copy-start.3
  107.9 74.2 %all-to-all-start.2 = ((bf16[8,384,256]{2,1,0:T(8,128)(2,1)}), bf16[8,384,256]{2,1,0:T(8,128)(2,1)S(1)}, u32[]{:S(2)}, u32[]{:S(2)}) async-start(bf16[8,384,256]{2,1,0:T(8,128)(2,1)} %bitcast.32), calls=%async_computation.2 | async-start | bytes 3145728 | tf_op jit(solution)/shard_map/all_to_all | solution.py:175
  182.2 1.2 copy-start.5
Sparse Core Ops, SparseCore 0:
  106.7 120.0 reduce-scatter.1
where the time goes:
time: 237 us; the launch traced here: 236 us
  waiting for transfers between devices  124 us (52%)
  Pallas kernels  32.8 us (14%)
  local copies, waits for them, and re-layouts  27.9 us (12%)
  between operations  14.1 us (6%)
  blocking collectives  13.6 us (6%)
  matrix products  8.44 us (4%)
  other arithmetic  7.5 us (3%)
  starting transfers between devices  7.2 us (3%)
    all_to_all x1, waiting for transfers between devices, shards(): lax.all_to_all(grad_table.astype(jnp.bfloat16).reshape(kv_count, capacity...  70.1 us
    reduce_scatter x1, waiting for transfers between devices, shards(): lax.psum_scatter(weight_part, 'kv', scatter_dimension=0, tiled=True)  40.4 us
    pallas_call x1, Pallas kernels, shards(): pl.pallas_call(functools.partial(attend, group_size), grid_spec=pltpu.Pre...  29.6 us
    all_to_all x1, waiting for transfers between devices, shards(): lax.all_to_all(fetched, 'kv', split_axis=0, concat_axis=0, tiled=True)  13.9 us
    all_to_all x1, blocking collectives, shards(): lax.all_to_all(request, 'kv', split_axis=0, concat_axis=0, tiled=True)  13.6 us
    unnamed x18, local copies, waits for them, and re-layouts  9 us
    dot_general x1, matrix products, shards(): lax.dot_general(inputs, query_grad, (((0,), (0,)), ((), ())), preferred_e...  8.44 us
  transfers between devices with their start and end apart: 3, of which 3 were waited for; matrix products, arithmetic and copies ran while one was open for 10% of the time, Pallas kernels for 1%

commit v1 on v0

v1 whole, which is shorter than its diff:
```python
import functools

import jax
import jax.numpy as jnp
from jax import lax
from jax.experimental import pallas as pl
from jax.experimental.pallas import tpu as pltpu
from jax.sharding import PartitionSpec as P

DH = 64
BLK = 64
QB = 128
NSEL = 16
CHUNK = 4
SCALE = DH ** (-0.5)
MESH = pl.DeviceIdType.MESH
SUBS = 4


def whole(n, kv_heads, group, tok, start_ref, first_ref, pos_ref, q_ref, do_ref, ls_ref, kv_hbm, inp_hbm,
          dq_ref, kvg_ref, wg_ref, *scratch):
    it = iter(scratch)
    tabs = [next(it) for _ in range(kv_heads)]
    qts = [next(it) for _ in range(kv_heads)]
    owns = [next(it) for _ in range(kv_heads)]
    ysend = [next(it) for _ in range(kv_heads)]
    yrecv = [next(it) for _ in range(kv_heads)]
    zsend = [next(it) for _ in range(kv_heads)]
    zrecv = [next(it) for _ in range(kv_heads)]
    rsend = [next(it) for _ in range(kv_heads)]
    rrecv = [next(it) for _ in range(kv_heads)]
    inp, w1, kv_scr, p_scr, dp_scr, a_scr, both_scr = [next(it) for _ in range(7)]
    (inp_sem, own_sem, fz_s, fy_s, f_r, gy_s, gy_r, gz_s, gz_r, r_s, r_r) = [next(it) for _ in range(11)]

    rows_n = n // 2
    nqb = tok // QB
    nblk = tok // BLK
    lanes = group * QB
    width = group * DH
    sub_w = width // SUBS
    me = lax.axis_index("kv")
    r, c = me // 2, me % 2
    partner = 2 * r + 1 - c
    up, down = me + 2, me - 2
    has_up, has_down = r < rows_n - 1, r > 0

    def at_pos(p):
        p = lax.rem(p + 2 * n, n)
        return jnp.where(p < rows_n, 2 * p, 2 * (n - 1 - p) + 1)

    pos_me = jnp.where(c == 0, r, n - 1 - r)
    ring_to = (at_pos(pos_me + 1), at_pos(pos_me - 1))

    barrier = pltpu.get_barrier_semaphore()
    pl.semaphore_signal(barrier, inc=1, device_id={"kv": partner}, device_id_type=MESH)

    @pl.when(has_up)
    def _():
        pl.semaphore_signal(barrier, inc=1, device_id={"kv": up}, device_id_type=MESH)

    @pl.when(has_down)
    def _():
        pl.semaphore_signal(barrier, inc=1, device_id={"kv": down}, device_id_type=MESH)

    own_rows = pl.ds(me * nblk, nblk)
    own_cp = [
        pltpu.make_async_copy(kv_hbm.at[:, :, h * 2 * DH:(h + 1) * 2 * DH], tabs[h].at[own_rows], own_sem.at[h])
        for h in range(kv_heads)
    ]
    for cp in own_cp:
        cp.start()
    drow = inp_hbm.shape[1] // n
    inp_cp = [
        pltpu.make_async_copy(inp_hbm.at[:, i * drow:(i + 1) * drow], inp.at[i], inp_sem.at[i]) for i in range(n)
    ]
    for cp in inp_cp:
        cp.start()
    w1[...] = jnp.zeros_like(w1)
    both_scr[nqb * NSEL] = jnp.zeros((BLK, 2 * DH), jnp.float32)
    for cp in own_cp:
        cp.wait()
    pl.semaphore_wait(barrier, 1 + has_up.astype(jnp.int32) + has_down.astype(jnp.int32))

    def fetch(h, owner, sems, slot, target):
        rows = pl.ds(owner * nblk, nblk)
        return pltpu.make_async_remote_copy(
            src_ref=tabs[h].at[rows], dst_ref=tabs[h].at[rows], send_sem=sems.at[h, slot],
            recv_sem=f_r.at[h, owner], device_id={"kv": target}, device_id_type=MESH)

    def forward(h, k):
        owner = 2 * (r - k) + c

        @pl.when(r >= k)
        def _():
            if k > 0:
                fetch(h, owner, fz_s, k, partner).wait_recv()

            @pl.when(has_up)
            def _():
                fetch(h, owner, fz_s, k, up).start()

            @pl.when((c == 0) if k == 0 else (c >= 0))
            def _():
                fetch(h, owner, fy_s, k, partner).start()

    def arrived(h):
        for k in range(rows_n):
            @pl.when((r >= k) if k > 0 else (c == 1))
            def _():
                fetch(h, 2 * (r - k) + 1 - c, fy_s, k, partner).wait_recv()

    def attend(h, qb):
        tab = tabs[h]
        qrow = pl.ds(pl.multiple_of(qb * QB, QB), QB)
        cols = slice(h * width, (h + 1) * width)
        q_t = (q_ref[qrow, cols].astype(jnp.float32) * SCALE).T.astype(jnp.bfloat16)
        do_t = do_ref[qrow, cols].astype(jnp.float32).T.astype(jnp.bfloat16)
        for g in range(group):
            w1[:DH, g * QB:(g + 1) * QB] = q_t[g * DH:(g + 1) * DH]
            w1[DH:, lanes + g * QB:lanes + (g + 1) * QB] = do_t[g * DH:(g + 1) * DH]
        for j in range(NSEL):
            kv_scr[j * BLK:(j + 1) * BLK, :] = tab[start_ref[qb, j]]
        rows = CHUNK * BLK
        lane = lax.broadcasted_iota(jnp.int32, (1, lanes), 1)
        qpos = (me * nqb + qb) * QB + lax.rem(lane, QB)
        within = lax.broadcasted_iota(jnp.int32, (BLK, lanes), 0)
        sums = ls_ref[h * nqb + qb]
        delta = jnp.zeros((1, lanes), jnp.float32)
        for ch in range(NSEL // CHUNK):
            kv = kv_scr[ch * rows:(ch + 1) * rows, :]
            scores = jnp.dot(kv, w1[:, :lanes], preferred_element_type=jnp.float32)
            grads = jnp.dot(kv, w1[:, lanes:], preferred_element_type=jnp.float32)
            for i in range(CHUNK):
                last = qpos - first_ref[qb, ch * CHUNK + i]
                here = slice(i * BLK, (i + 1) * BLK)
                there = slice(ch * rows + i * BLK, ch * rows + (i + 1) * BLK)
                prob = jnp.where(within <= last, jnp.exp(scores[here] - sums), jnp.float32(0.0))
                rounded = prob.astype(jnp.bfloat16)
                delta += jnp.sum(rounded.astype(jnp.float32) * grads[here], axis=0, keepdims=True)
                p_scr[there, :] = prob
                dp_scr[there, :] = grads[here]
                a_scr[there, lanes:] = rounded
        for ch in range(NSEL // CHUNK):
            there = slice(ch * rows, (ch + 1) * rows)
            a_scr[there, :lanes] = (p_scr[there, :] * (dp_scr[there, :] - delta)).astype(jnp.bfloat16)
            both_scr[pl.ds(qb * NSEL + ch * CHUNK, CHUNK)] = lax.dot_general(
                a_scr[there, :], w1[...], (((1,), (1,)), ((), ())), preferred_element_type=jnp.float32
            ).reshape(CHUNK, BLK, 2 * DH)
        dq_t = jnp.dot(kv_scr[...].T, a_scr[:, :lanes], preferred_element_type=jnp.float32)[:DH] * SCALE
        stacked = jnp.concatenate([dq_t[:, g * QB:(g + 1) * QB] for g in range(group)], axis=0)
        qts[h][qb] = stacked.astype(jnp.bfloat16)
        dq_ref[qrow, cols] = stacked.T.astype(jnp.bfloat16)

    def block_sum(block):
        total = None
        for qb in range(nqb):
            part = both_scr[pos_ref[qb, block]]
            total = part if total is None else total + part
        return total

    def gsend(h, row):
        return pltpu.make_async_remote_copy(
            src_ref=ysend[h].at[row], dst_ref=yrecv[h].at[row], send_sem=gy_s.at[h, row],
            recv_sem=gy_r.at[h, row], device_id={"kv": partner}, device_id_type=MESH)

    def zcopy(h, row):
        return pltpu.make_async_remote_copy(
            src_ref=zsend[h].at[row], dst_ref=zrecv[h].at[row], send_sem=gz_s.at[h, row],
            recv_sem=gz_r.at[h, row], device_id={"kv": down}, device_id_type=MESH)

    def give(h):
        def other(row, carry):
            def one(k, inner):
                block = (2 * row + 1 - c) * nblk + k
                ysend[h][row, pl.ds(pl.multiple_of(k * BLK, BLK), BLK), :] = block_sum(block).astype(jnp.bfloat16)
                return inner

            lax.fori_loop(0, nblk, one, 0)
            gsend(h, row).start()
            return carry

        lax.fori_loop(0, r + c, other, 0)

        def mine(row, carry):
            def one(k, inner):
                block = (2 * row + c) * nblk + k
                owns[h][row, pl.ds(pl.multiple_of(k * BLK, BLK), BLK), :] = block_sum(block)
                return inner

            lax.fori_loop(0, nblk, one, 0)
            return carry

        lax.fori_loop(0, r + 1, mine, 0)

    def pass_down(h, row):
        gsend(h, row).wait_recv()

        @pl.when(has_up)
        def _():
            zcopy(h, row).wait_recv()
            zsend[h][row] = (
                owns[h][row] + yrecv[h][row].astype(jnp.float32) + zrecv[h][row].astype(jnp.float32)
            ).astype(jnp.bfloat16)

        @pl.when(jnp.logical_not(has_up))
        def _():
            zsend[h][row] = (owns[h][row] + yrecv[h][row].astype(jnp.float32)).astype(jnp.bfloat16)

        zcopy(h, row).start()

    def pass_all(h):
        def step(row, carry):
            pass_down(h, row)
            return carry

        lax.fori_loop(0, r, step, 0)

    def keep(h):
        cols = slice(h * 2 * DH, (h + 1) * 2 * DH)
        kvg_ref[:, cols] = owns[h][r]

        @pl.when(c == 0)
        def _():
            gsend(h, r).wait_recv()
            kvg_ref[:, cols] += yrecv[h][r].astype(jnp.float32)

        @pl.when(has_up)
        def _():
            zcopy(h, r).wait_recv()
            kvg_ref[:, cols] += zrecv[h][r].astype(jnp.float32)

    def rcopy(h, u, s):
        return pltpu.make_async_remote_copy(
            src_ref=rsend[h].at[u, s], dst_ref=rrecv[h].at[u, s], send_sem=r_s.at[h, u, s],
            recv_sem=r_r.at[h, u, s], device_id={"kv": ring_to[u * 2 // SUBS]}, device_id_type=MESH)

    half = width // 2

    def partial_of(h, d, target):
        chunk = inp[target]
        total = None
        for qb in range(nqb):
            part = jnp.dot(qts[h][qb, d * half:(d + 1) * half, :], chunk[qb * QB:(qb + 1) * QB, :],
                           preferred_element_type=jnp.float32)
            total = part if total is None else total + part
        return total

    def ring(h, s, first):
        for d in range(2):
            target = at_pos(pos_me - 1 - s) if d == 0 else at_pos(pos_me + 1 + s)
            part = partial_of(h, d, target)
            for v in range(SUBS // 2):
                u = d * (SUBS // 2) + v
                piece = part[v * sub_w:(v + 1) * sub_w]
                if not first:
                    rcopy(h, u, s - 1).wait_recv()
                    piece = piece + rrecv[h][u, s - 1].astype(jnp.float32)
                rsend[h][u, s] = piece.astype(jnp.bfloat16)
                rcopy(h, u, s).start()

    def ring_end(h):
        for d in range(2):
            part = partial_of(h, d, me)
            got = []
            for v in range(SUBS // 2):
                u = d * (SUBS // 2) + v
                rcopy(h, u, n - 2).wait_recv()
                got.append(part[v * sub_w:(v + 1) * sub_w] + rrecv[h][u, n - 2].astype(jnp.float32))
            wg_ref[:, h * width + d * half:h * width + (d + 1) * half] = jnp.concatenate(got, axis=0).T

    for h in range(kv_heads):
        forward(h, 0)
    for k in range(1, rows_n):
        forward(0, k)
    arrived(0)

    late = kv_heads > 1
    done = 0
    for h in range(kv_heads):
        def loop(qb, carry, h=h):
            attend(h, qb)
            if h + 1 < kv_heads:
                for k in range(1, rows_n):
                    @pl.when(qb == min(k - 1, nqb - 1))
                    def _():
                        forward(h + 1, k)
            return carry

        lax.fori_loop(0, nqb, loop, 0)
        give(h)
        if h == 0:
            for cp in inp_cp:
                cp.wait()
        ring(h, 0, True)
        if h + 1 < kv_heads:
            arrived(h + 1)

    for h in range(kv_heads):
        pass_all(h)

    def ring_loop(s, carry):
        for h in range(kv_heads):
            ring(h, s, False)
        return carry

    lax.fori_loop(1, n - 1, ring_loop, 0)
    for h in range(kv_heads):
        keep(h)
        ring_end(h)

    for h in range(kv_heads):
        for k in range(rows_n):
            @pl.when((r >= k) & has_up)
            def _():
                fetch(h, 2 * (r - k) + c, fz_s, k, up).wait_send()

            @pl.when((r >= k) if k > 0 else (c == 0))
            def _():
                fetch(h, 2 * (r - k) + c, fy_s, k, partner).wait_send()

        def drain_y(row, carry, h=h):
            gsend(h, row).wait_send()
            return carry

        def drain_z(row, carry, h=h):
            zcopy(h, row).wait_send()
            return carry

        lax.fori_loop(0, r + c, drain_y, 0)
        lax.fori_loop(0, r, drain_z, 0)

        def drain_r(s, carry, h=h):
            for u in range(SUBS):
                rcopy(h, u, s).wait_send()
            return carry

        lax.fori_loop(0, n - 1, drain_r, 0)


def shards(queries, keys_values, log_sums, out_grad, inputs, chosen):
    tok = queries.shape[0]
    heads_here = queries.shape[1] // DH
    kv_heads = keys_values.shape[1] // (2 * DH)
    group = heads_here // kv_heads
    nqb, nblk = tok // QB, tok // BLK
    n = lax.axis_size("kv")
    rows_n = n // 2
    lanes = group * QB
    width = group * DH
    sub_w = width // SUBS
    drow = inputs.shape[1] // n
    flat = jnp.arange(nqb * NSEL, dtype=jnp.int32).reshape(nqb, NSEL)
    one_hot = chosen[:, None, :] == jnp.arange(n * nblk, dtype=jnp.int32)[None, :, None]
    zero_at = nqb * NSEL
    pos = zero_at + jnp.sum(jnp.where(one_hot, flat[:, None, :] - zero_at, 0), axis=2)
    start = jnp.maximum(chosen, 0)
    first = jnp.where(chosen >= 0, chosen * BLK, 1 << 30)
    sums = (
        log_sums.reshape(nqb, QB, kv_heads, group).transpose(2, 0, 3, 1).reshape(kv_heads * nqb, 1, lanes)
    )
    vmem = pl.BlockSpec(memory_space=pltpu.VMEM)
    smem = pl.BlockSpec(memory_space=pltpu.SMEM)
    hbm = pl.BlockSpec(memory_space=pl.ANY)
    per_head = lambda shape, dtype: [pltpu.VMEM(shape, dtype)] * kv_heads
    bf, f32 = jnp.bfloat16, jnp.float32
    keys = NSEL * BLK
    dma = pltpu.SemaphoreType.DMA
    scratch = (
        per_head((n * nblk, BLK, 2 * DH), bf)
        + per_head((nqb, width, QB), bf)
        + per_head((rows_n, tok, 2 * DH), f32)
        + per_head((rows_n, tok, 2 * DH), bf)
        + per_head((rows_n, tok, 2 * DH), bf)
        + per_head((rows_n, tok, 2 * DH), bf)
        + per_head((rows_n, tok, 2 * DH), bf)
        + per_head((SUBS, n - 1, sub_w, drow), bf)
        + per_head((SUBS, n - 1, sub_w, drow), bf)
        + [
            pltpu.VMEM((n, tok, drow), bf),
            pltpu.VMEM((2 * DH, 2 * lanes), bf),
            pltpu.VMEM((keys, 2 * DH), bf),
            pltpu.VMEM((keys, lanes), f32),
            pltpu.VMEM((keys, lanes), f32),
            pltpu.VMEM((keys, 2 * lanes), bf),
            pltpu.VMEM((nqb * NSEL + 1, BLK, 2 * DH), f32),
            dma((n,)),
            dma((kv_heads,)),
            dma((kv_heads, rows_n)),
            dma((kv_heads, rows_n)),
            dma((kv_heads, n)),
            dma((kv_heads, rows_n)),
            dma((kv_heads, rows_n)),
            dma((kv_heads, rows_n)),
            dma((kv_heads, rows_n)),
            dma((kv_heads, SUBS, n - 1)),
            dma((kv_heads, SUBS, n - 1)),
        ]
    )
    return pl.pallas_call(
        functools.partial(whole, n, kv_heads, group, tok),
        in_specs=[smem, smem, smem, vmem, vmem, vmem, hbm, hbm],
        out_specs=[vmem, vmem, vmem],
        out_shape=[
            jax.ShapeDtypeStruct((tok, heads_here * DH), bf),
            jax.ShapeDtypeStruct((tok, kv_heads * 2 * DH), f32),
            jax.ShapeDtypeStruct((drow, heads_here * DH), f32),
        ],
        scratch_shapes=scratch,
        compiler_params=pltpu.CompilerParams(
            collective_id=0, has_side_effects=True, vmem_limit_bytes=63 * 1024 * 1024
        ),
    )(start, first, pos.astype(jnp.int32), queries, out_grad, sums, keys_values.reshape(nblk, BLK, -1), inputs)


def solution(mesh):
    in_specs = (
        P("kv", "tp"),
        P("kv", "tp"),
        P("kv", "tp"),
        P("kv", "tp"),
        P("kv", None),
        P("kv", None),
    )
    out_specs = (P("kv", "tp"), P("kv", "tp"), P("kv", "tp"))
    return jax.shard_map(shards, mesh=mesh, in_specs=in_specs, out_specs=out_specs, check_vma=False)
```

time: 237 us -> 141 us (0.59)
  waiting for transfers between devices: 124 us -> 0 us
  Pallas kernels: 32.8 us -> 129 us
  local copies, waits for them, and re-layouts: 27.9 us -> 7.74 us
  blocking collectives: 13.6 us -> 0 us
  between operations: 14.1 us -> 0.65 us
  matrix products: 8.44 us -> 0 us
  starting transfers between devices: 7.2 us -> 0 us
  other arithmetic: 7.5 us -> 2.67 us
    pallas_call x2 -> x1, Pallas kernels: 32.8 us -> 129 us  [shards(): pl.pallas_call(functools.partial(whole, n, kv_heads, group, tok), in_spec...]
    all_to_all x2 -> x0, waiting for transfers between devices: 83.9 us -> none  [the longest x1 70.1 us: shards(): lax.all_to_all(grad_table.astype(jnp.bfloat16).reshape(kv_count, capacity...]
    reduce_scatter x1 -> x0, waiting for transfers between devices: 40.4 us -> none  [shards(): lax.psum_scatter(weight_part, 'kv', scatter_dimension=0, tiled=True)]
    all_to_all x1 -> x0, blocking collectives: 13.6 us -> none  [shards(): lax.all_to_all(request, 'kv', split_axis=0, concat_axis=0, tiled=True)]
    transpose x4 -> x1, local copies, waits for them, and re-layouts: 9.96 us -> 0.61 us  [shards(): log_sums.reshape(nqb, QB, kv_heads, group).transpose(2, 0, 3, 1)]
    dot_general x1 -> x0, matrix products: 8.44 us -> none  [shards(): lax.dot_general(inputs, query_grad, (((0,), (0,)), ((), ())), preferred_e...]
    all_to_all x2 -> x0, starting transfers between devices: 7.16 us -> none  [the longest x1 3.58 us: shards(): lax.all_to_all(fetched, 'kv', split_axis=0, concat_axis=0, tiled=True)]
    concatenate x1 -> x0, other arithmetic: 4.46 us -> none  [shards(): jnp.concatenate([jnp.pad(query_rows, pad + ((0, DH),)), jnp.pad(grad_rows...]
  transfers between devices with their start and end apart: 3 -> 0, of which waited for: 3 -> 0; matrix products, arithmetic and copies ran while one was open for 10% -> 0% of each run, Pallas kernels for 1% -> 0%
where the time goes in v1:
time: 141 us; the launch traced here: 140 us
  Pallas kernels  129 us (91%)
  local copies, waits for them, and re-layouts  7.74 us (5%)
  other arithmetic  2.67 us (2%)
    pallas_call x1, Pallas kernels, shards(): pl.pallas_call(functools.partial(whole, n, kv_heads, group, tok), in_spec...  129 us
    unnamed x3, local copies, waits for them, and re-layouts  6.39 us

profile of v1, /device:TPU:0, one launch (start us, length us, event | category | flops | bytes accessed | tf_op | source)
XLA Modules:
  0.0 140.4 jit_solution(2137127095875975038)
XLA Ops:
  0.6 0.8 select_reduce_fusion
  1.4 0.6 broadcast_add_fusion.pos_ref
  2.0 1.3 multiply_select_fusion
  3.3 0.7 reshape.31
  4.1 0.6 copy.11
  4.7 129.3 %shard_map.85 = (bf16[768,512]{1,0:T(8,128)(2,1)}, f32[768,256]{1,0:T(8,128)}, f32[512,512]{1,0:T(8,128)}) custom-call(s32[6,16]{1,0:T(8,128)} %get-tuple-element.4.start_ref, s32[6,16]{1,0:T(8,128)} %get-tuple-element.3.first_ref, s32[6,96]{1,0:T(8,128)} %broadcast_add_fusion.pos_ref, bf16[768,512]{1,0:T(8,128)(2,1)} %q_ref.1, bf16[768,512]{1,0:T(8,128)(2,1)} %do_ref.1, ...), custom_call_target="tpu_custom_call" | custom-call | tf_op jit(solution)/shard_map/pallas_call | solution.py:399
  134.0 2.1 %copy.15 = bf16[768,512]{1,0:T(8,128)(2,1)} copy(bf16[768,512]{1,0:T(8,128)(2,1)} %get-tuple-element.8) | data formatting | bytes 1572864
  136.0 2.1 %copy.16 = f32[768,256]{1,0:T(8,128)} copy(f32[768,256]{1,0:T(8,128)} %get-tuple-element.9) | data formatting | bytes 1572864
  138.1 2.3 %copy.17 = f32[512,512]{1,0:T(8,128)} copy(f32[512,512]{1,0:T(8,128)} %get-tuple-element.10) | data formatting | bytes 2097152
  (1 shorter events, 0.0 us)

commit v2 on v1

v2 whole, which is shorter than its diff:
```python
import functools

import jax
import jax.numpy as jnp
from jax import lax
from jax.experimental import pallas as pl
from jax.experimental.pallas import tpu as pltpu
from jax.sharding import PartitionSpec as P

DH = 64
BLK = 64
QB = 128
NSEL = 16
CHUNK = 4
SCALE = DH ** (-0.5)
MESH = pl.DeviceIdType.MESH
SUBS = 4
PIECES = 2


def whole(n, kv_heads, group, tok, chosen_ref, list_ref, ls_ref, q_hbm, do_hbm, kv_hbm, inp_hbm,
          dq_hbm, kvg_hbm, wg_hbm, *scratch):
    it = iter(scratch)
    tabs = [next(it) for _ in range(kv_heads)]
    qts = [next(it) for _ in range(kv_heads)]
    owns = [next(it) for _ in range(kv_heads)]
    rows_n = n // 2
    arr = [[next(it) for _ in range(rows_n)] for _ in range(kv_heads)]
    stage = [[next(it) for _ in range(rows_n)] for _ in range(kv_heads)]
    ysend = [next(it) for _ in range(kv_heads)]
    yrecv = [[next(it) for _ in range(rows_n)] for _ in range(kv_heads)]
    zsend = [next(it) for _ in range(kv_heads)]
    zrecv = [next(it) for _ in range(kv_heads)]
    rsend = [next(it) for _ in range(kv_heads)]
    rrecv = [next(it) for _ in range(kv_heads)]
    inp, w1, kv_scr, p_scr, dp_scr, a_scr, both_scr = [next(it) for _ in range(7)]
    q_ref, do_ref, ls_t, dq_ref, kvg_ref, wg_ref, table_v, pos_v, req_v, plist_v, pch_v = [next(it) for _ in range(11)]
    table, pos_ref, req_ref, pch_ref = [next(it) for _ in range(4)]
    (inp_sem, own_sem, in_sem, tab_sem, out_sem, list_sem, loc_sem, fz_s, fy_s, fy_r, f_r, gy_s, gy_r, gz_s, gz_r, r_s, r_r) = [next(it) for _ in range(17)]

    nqb = tok // QB
    nblk = tok // BLK
    cap = nblk // 2
    blocks = n * nblk
    compact = rows_n * nblk
    lanes = group * QB
    width = group * DH
    sub_w = width // SUBS
    me = lax.axis_index("kv")
    r, c = me // 2, me % 2
    partner = 2 * r + 1 - c
    up, down = me + 2, me - 2
    has_up, has_down = r < rows_n - 1, r > 0

    def at_pos(p):
        p = lax.rem(p + 2 * n, n)
        return jnp.where(p < rows_n, 2 * p, 2 * (n - 1 - p) + 1)

    pos_me = jnp.where(c == 0, r, n - 1 - r)
    ring_to = (at_pos(pos_me + 1), at_pos(pos_me - 1))

    barrier = pltpu.get_barrier_semaphore()
    pl.semaphore_signal(barrier, inc=1, device_id={"kv": partner}, device_id_type=MESH)

    @pl.when(has_up)
    def _():
        pl.semaphore_signal(barrier, inc=1, device_id={"kv": up}, device_id_type=MESH)

    @pl.when(has_down)
    def _():
        pl.semaphore_signal(barrier, inc=1, device_id={"kv": down}, device_id_type=MESH)

    own_cp = [
        pltpu.make_async_copy(kv_hbm.at[:, :, h * 2 * DH:(h + 1) * 2 * DH], arr[h][0], own_sem.at[h])
        for h in range(kv_heads)
    ]
    for cp in own_cp:
        cp.start()
    drow = inp_hbm.shape[1] // n
    inp_cp = [
        pltpu.make_async_copy(inp_hbm.at[:, i * drow:(i + 1) * drow], inp.at[i], inp_sem.at[i]) for i in range(n)
    ]
    for cp in inp_cp:
        cp.start()
    in_cp = [
        pltpu.make_async_copy(q_hbm, q_ref, in_sem.at[0]),
        pltpu.make_async_copy(do_hbm, do_ref, in_sem.at[1]),
    ]
    for cp in in_cp:
        cp.start()
    for cp in own_cp:
        cp.wait()
    pl.semaphore_wait(barrier, 1 + has_up.astype(jnp.int32) + has_down.astype(jnp.int32))

    piece_n = nblk // PIECES

    def zfetch(h, k, f):
        src = arr[h][k].at[f * piece_n:(f + 1) * piece_n]
        dst = arr[h][min(k + 1, rows_n - 1)].at[f * piece_n:(f + 1) * piece_n]
        return pltpu.make_async_remote_copy(
            src_ref=src, dst_ref=dst, send_sem=fz_s.at[h, f, k], recv_sem=f_r.at[h, f, min(k + 1, rows_n - 1)],
            device_id={"kv": up}, device_id_type=MESH)

    def yfetch(h, k):
        return pltpu.make_async_remote_copy(
            src_ref=stage[h][k], dst_ref=tabs[h].at[pl.ds(compact + (r - k) * cap, cap)], send_sem=fy_s.at[h, k],
            recv_sem=fy_r.at[h, k], device_id={"kv": partner}, device_id_type=MESH)

    def local(h, k):
        return pltpu.make_async_copy(arr[h][k], tabs[h].at[pl.ds((r - k) * nblk, nblk)], loc_sem.at[h, k])

    def forward(h, k, f):
        @pl.when(r >= k)
        def _():
            if k > 0:
                zfetch(h, k - 1, f).wait_recv()
            if k < rows_n - 1:
                @pl.when(has_up)
                def _():
                    zfetch(h, k, f).start()

    def across(h, k):
        @pl.when(r >= k)
        def _():
            local(h, k).start()

            @pl.when((c == 0) if k == 0 else (c >= 0))
            def _():
                owner = 2 * (r - k) + c
                for i in range(cap):
                    stage[h][k][i] = arr[h][k][req_ref[n + owner, i]]
                yfetch(h, k).start()

    def arrived(h):
        for k in range(rows_n):
            @pl.when((r >= k) if k > 0 else (c == 1))
            def _():
                yfetch(h, k).wait_recv()

            @pl.when(r >= k)
            def _():
                local(h, k).wait()

    def attend(h, qb):
        tab = tabs[h]
        qrow = pl.ds(pl.multiple_of(qb * QB, QB), QB)
        cols = slice(h * width, (h + 1) * width)
        q_t = (q_ref[qrow, cols].astype(jnp.float32) * SCALE).T.astype(jnp.bfloat16)
        do_t = do_ref[qrow, cols].astype(jnp.float32).T.astype(jnp.bfloat16)
        for g in range(group):
            w1[:DH, g * QB:(g + 1) * QB] = q_t[g * DH:(g + 1) * DH]
            w1[DH:, lanes + g * QB:lanes + (g + 1) * QB] = do_t[g * DH:(g + 1) * DH]
        for j in range(NSEL):
            kv_scr[j * BLK:(j + 1) * BLK, :] = tab[pos_ref[nqb, table[qb, j]]]
        rows = CHUNK * BLK
        lane = lax.broadcasted_iota(jnp.int32, (1, lanes), 1)
        qpos = (me * nqb + qb) * QB + lax.rem(lane, QB)
        within = lax.broadcasted_iota(jnp.int32, (BLK, lanes), 0)
        sums = jnp.concatenate([ls_t[qb, h * group + g:h * group + g + 1, :] for g in range(group)], axis=1)
        delta = jnp.zeros((1, lanes), jnp.float32)
        for ch in range(NSEL // CHUNK):
            kv = kv_scr[ch * rows:(ch + 1) * rows, :]
            scores = jnp.dot(kv, w1[:, :lanes], preferred_element_type=jnp.float32)
            grads = jnp.dot(kv, w1[:, lanes:], preferred_element_type=jnp.float32)
            for i in range(CHUNK):
                last = qpos - table[qb, NSEL + ch * CHUNK + i]
                here = slice(i * BLK, (i + 1) * BLK)
                there = slice(ch * rows + i * BLK, ch * rows + (i + 1) * BLK)
                prob = jnp.where(within <= last, jnp.exp(scores[here] - sums), jnp.float32(0.0))
                rounded = prob.astype(jnp.bfloat16)
                delta += jnp.sum(rounded.astype(jnp.float32) * grads[here], axis=0, keepdims=True)
                p_scr[there, :] = prob
                dp_scr[there, :] = grads[here]
                a_scr[there, lanes:] = rounded
        for ch in range(NSEL // CHUNK):
            there = slice(ch * rows, (ch + 1) * rows)
            a_scr[there, :lanes] = (p_scr[there, :] * (dp_scr[there, :] - delta)).astype(jnp.bfloat16)
            both_scr[pl.ds(qb * NSEL + ch * CHUNK, CHUNK)] = lax.dot_general(
                a_scr[there, :], w1[...], (((1,), (1,)), ((), ())), preferred_element_type=jnp.float32
            ).reshape(CHUNK, BLK, 2 * DH)
        dq_t = jnp.dot(kv_scr[...].T, a_scr[:, :lanes], preferred_element_type=jnp.float32)[:DH] * SCALE
        stacked = jnp.concatenate([dq_t[:, g * QB:(g + 1) * QB] for g in range(group)], axis=0)
        qts[h][qb] = stacked.astype(jnp.bfloat16)
        dq_ref[qrow, cols] = stacked.T.astype(jnp.bfloat16)

    def block_sum(block):
        total = None
        for qb in range(nqb):
            part = both_scr[pos_ref[qb, block]]
            total = part if total is None else total + part
        return total

    def gsend(h, row):
        return pltpu.make_async_remote_copy(
            src_ref=ysend[h].at[row], dst_ref=yrecv[h][row].at[:cap], send_sem=gy_s.at[h, row],
            recv_sem=gy_r.at[h, row], device_id={"kv": partner}, device_id_type=MESH)

    def zcopy(h, row):
        return pltpu.make_async_remote_copy(
            src_ref=zsend[h].at[row], dst_ref=zrecv[h].at[row], send_sem=gz_s.at[h, row],
            recv_sem=gz_r.at[h, row], device_id={"kv": down}, device_id_type=MESH)

    def give(h):
        for row in range(rows_n):
            @pl.when(row < r + c)
            def _():
                def one(k, inner):
                    owner = 2 * row + 1 - c
                    ysend[h][row, k] = block_sum(owner * nblk + req_ref[owner, k]).astype(jnp.bfloat16)
                    return inner

                lax.fori_loop(0, cap, one, 0)
                gsend(h, row).start()

        def mine(i, carry):
            row, k = i // nblk, i % nblk
            owns[h][row, k] = block_sum((2 * row + c) * nblk + k)
            return carry

        lax.fori_loop(0, (r + 1) * nblk, mine, 0)

    def pass_down(h, row):
        gsend(h, row).wait_recv()

        @pl.when(has_up)
        def _():
            zcopy(h, row).wait_recv()

        def one(k, carry):
            total = owns[h][row, k] + yrecv[h][row][pos_ref[nqb + 1, (2 * row + c) * nblk + k]].astype(jnp.float32)

            @pl.when(has_up)
            def _():
                zsend[h][row, k] = (total + zrecv[h][row, k].astype(jnp.float32)).astype(jnp.bfloat16)

            @pl.when(jnp.logical_not(has_up))
            def _():
                zsend[h][row, k] = total.astype(jnp.bfloat16)

            return carry

        lax.fori_loop(0, nblk, one, 0)
        zcopy(h, row).start()

    def keep(h):
        cols = slice(h * 2 * DH, (h + 1) * 2 * DH)

        @pl.when(has_up)
        def _():
            zcopy(h, r).wait_recv()
            kvg_ref[:, cols] = (owns[h][r] + zrecv[h][r].astype(jnp.float32)).reshape(tok, 2 * DH)

        @pl.when(jnp.logical_not(has_up))
        def _():
            kvg_ref[:, cols] = owns[h][r].reshape(tok, 2 * DH)

        for row in range(rows_n):
            @pl.when((c == 0) & (r == row))
            def _():
                gsend(h, row).wait_recv()
                for k in range(nblk):
                    kvg_ref[k * BLK:(k + 1) * BLK, cols] += (
                        yrecv[h][row][pos_ref[nqb + 1, (2 * row + c) * nblk + k]].astype(jnp.float32))

    def rcopy(h, u, s):
        return pltpu.make_async_remote_copy(
            src_ref=rsend[h].at[u, s], dst_ref=rrecv[h].at[u, s], send_sem=r_s.at[h, u, s],
            recv_sem=r_r.at[h, u, s], device_id={"kv": ring_to[u * 2 // SUBS]}, device_id_type=MESH)

    half = width // 2

    def partial_of(h, d, target):
        chunk = inp[target]
        total = None
        for qb in range(nqb):
            part = jnp.dot(qts[h][qb, d * half:(d + 1) * half, :], chunk[qb * QB:(qb + 1) * QB, :],
                           preferred_element_type=jnp.float32)
            total = part if total is None else total + part
        return total

    def ring(h, s, first):
        for d in range(2):
            target = at_pos(pos_me - 1 - s) if d == 0 else at_pos(pos_me + 1 + s)
            part = partial_of(h, d, target)
            for v in range(SUBS // 2):
                u = d * (SUBS // 2) + v
                piece = part[v * sub_w:(v + 1) * sub_w]
                if not first:
                    rcopy(h, u, s - 1).wait_recv()
                    piece = piece + rrecv[h][u, s - 1].astype(jnp.float32)
                rsend[h][u, s] = piece.astype(jnp.bfloat16)
                rcopy(h, u, s).start()

    def ring_end():
        parts = [[partial_of(h, d, me) for d in range(2)] for h in range(kv_heads)]
        for h in range(kv_heads):
            for d in range(2):
                got = []
                for v in range(SUBS // 2):
                    u = d * (SUBS // 2) + v
                    rcopy(h, u, n - 2).wait_recv()
                    got.append(parts[h][d][v * sub_w:(v + 1) * sub_w] + rrecv[h][u, n - 2].astype(jnp.float32))
                wg_ref[:, h * width + d * half:h * width + (d + 1) * half] = jnp.concatenate(got, axis=0).T

    def pass_slot(h, slot):
        for row in range(rows_n - 1):
            @pl.when((slot - (rows_n - 1 - r) == row) & (row < r))
            def _():
                with jax.named_scope(f"pass{h}"):
                    pass_down(h, row)

    list_cp = pltpu.make_async_remote_copy(
        src_ref=list_ref, dst_ref=plist_v, send_sem=list_sem.at[0], recv_sem=list_sem.at[1],
        device_id={"kv": partner}, device_id_type=MESH)
    list_cp.start()

    def ranks(ref, ids, within):
        need = ids == ref[0, 0]
        for qb in range(nqb):
            for j in range(NSEL):
                need = need | (ids == ref[qb, j])
        need = need.astype(jnp.int32)
        rank = jnp.zeros_like(need)
        for d in range(1, nblk):
            rank = rank + jnp.where(within >= d, pltpu.roll(need, d, 1), 0)
        return need, rank

    def wanted(need, rank, within, owner):
        out = jnp.zeros((n, 128), jnp.int32)
        lane = lax.broadcasted_iota(jnp.int32, (n, 128), 1)
        here = owner == lax.broadcasted_iota(jnp.int32, (n, pos_v.shape[1]), 0)
        for k in range(cap):
            hit = here & (need == 1) & (rank == k)
            out = jnp.where(lane == k, jnp.sum(jnp.where(hit, within, 0), axis=1, keepdims=True), out)
        return out

    with jax.named_scope("fetch_first"):
        for h in range(kv_heads):
            for f in range(PIECES):
                forward(h, 0, f)
        ids = lax.broadcasted_iota(jnp.int32, (1, pos_v.shape[1]), 1)
        owner = jnp.zeros_like(ids)
        for o in range(1, n):
            owner = owner + (ids >= o * nblk).astype(jnp.int32)
        within = ids - owner * nblk
        line = owner // 2
        own_col = owner - 2 * line == c
        need, rank = ranks(chosen_ref, ids, within)
        pos_v[nqb:nqb + 1, :] = jnp.where(own_col, line * nblk + within, compact + line * cap + rank)
        req_v[:n] = wanted(need, rank, within, owner)
        listed = list_ref[...]
        table_v[:nqb, :NSEL] = jnp.maximum(listed, 0)
        table_v[:nqb, NSEL:2 * NSEL] = jnp.where(listed >= 0, listed * BLK, 1 << 30)
        for qb in range(nqb):
            at = jnp.full(ids.shape, nqb * NSEL, jnp.int32)
            for j in range(NSEL):
                at = jnp.where(ids == chosen_ref[qb, j], qb * NSEL + j, at)
            pos_v[qb:qb + 1, :] = at
        list_cp.wait_recv()
        pch_v[:nqb, :NSEL] = plist_v[...]
        cp = pltpu.make_async_copy(pch_v, pch_ref, tab_sem.at[0])
        cp.start()
        cp.wait()
        need, rank = ranks(pch_ref, ids, within)
        pos_v[nqb + 1:nqb + 2, :] = jnp.where(need == 1, rank, cap)
        req_v[n:] = wanted(need, rank, within, owner)
        tab_cp = [
            pltpu.make_async_copy(table_v, table, tab_sem.at[0]),
            pltpu.make_async_copy(pos_v, pos_ref, tab_sem.at[1]),
            pltpu.make_async_copy(req_v, req_ref, tab_sem.at[2]),
        ]
        for cp in tab_cp:
            cp.start()
        for cp in tab_cp:
            cp.wait()
        for h in range(kv_heads):
            across(h, 0)
        for k in range(1, rows_n):
            for f in range(PIECES):
                forward(0, k, f)
            across(0, k)
            if k == 1:
                w1[...] = jnp.zeros_like(w1)
                both_scr[nqb * NSEL] = jnp.zeros((BLK, 2 * DH), jnp.float32)
                for h in range(kv_heads):
                    for row in range(rows_n):
                        yrecv[h][row][cap] = jnp.zeros((BLK, 2 * DH), jnp.bfloat16)
                for qb in range(nqb):
                    ls_t[qb] = ls_ref[:, qb * QB:(qb + 1) * QB]
        arrived(0)
        for cp in in_cp:
            cp.wait()

    early = [nqb // 2 if h + 1 < kv_heads else 0 for h in range(kv_heads)]
    pieces = [(k, f) for k in range(1, rows_n) for f in range(PIECES)]
    dq_cp = []
    for h in range(kv_heads):
        def loop(qb, carry, h=h):
            with jax.named_scope(f"attend{h}"):
                attend(h, qb)
            if h + 1 < kv_heads:
                for i, (k, f) in enumerate(pieces):
                    @pl.when(qb == i * nqb // len(pieces))
                    def _():
                        with jax.named_scope("forward_next"):
                            forward(h + 1, k, f)
                            if f == PIECES - 1:
                                across(h + 1, k)
            if h > 0:
                for k in range(early[h - 1]):
                    @pl.when(qb == 2 * k + 1)
                    def _():
                        with jax.named_scope(f"ring{h - 1}"):
                            ring(h - 1, k + 1, False)
                        pass_slot(h - 1, k)
            return carry

        lax.fori_loop(0, nqb, loop, 0)
        dq_cp.append(pltpu.make_async_copy(
            dq_ref.at[:, h * width:(h + 1) * width], dq_hbm.at[:, h * width:(h + 1) * width], out_sem.at[h]))
        dq_cp[h].start()
        if h == 0:
            for cp in inp_cp:
                cp.wait()
        with jax.named_scope(f"ring_first{h}"):
            ring(h, 0, True)
        with jax.named_scope(f"give{h}"):
            give(h)
        if h + 1 < kv_heads:
            with jax.named_scope("arrive_next"):
                arrived(h + 1)

    def ring_loop(s, carry):
        for h in range(kv_heads):
            @pl.when(s + early[h] <= n - 2)
            def _():
                with jax.named_scope(f"ring{h}"):
                    ring(h, s + early[h], False)
            pass_slot(h, s - 1 + early[h] if early[h] else s - 2)
        return carry

    lax.fori_loop(1, n - 1, ring_loop, 0)
    for h in range(kv_heads):
        with jax.named_scope(f"keep{h}"):
            keep(h)
    kvg_cp = pltpu.make_async_copy(kvg_ref, kvg_hbm, out_sem.at[kv_heads])
    kvg_cp.start()
    with jax.named_scope("ring_end"):
        ring_end()
    wg_cp = pltpu.make_async_copy(wg_ref, wg_hbm, out_sem.at[kv_heads + 1])
    wg_cp.start()

    list_cp.wait_send()
    for h in range(kv_heads):
        for k in range(rows_n):
            if k < rows_n - 1:
                @pl.when((r >= k) & has_up)
                def _():
                    for f in range(PIECES):
                        zfetch(h, k, f).wait_send()

            @pl.when((r >= k) if k > 0 else (c == 0))
            def _():
                yfetch(h, k).wait_send()

        for row in range(rows_n):
            @pl.when(row < r + c)
            def _():
                gsend(h, row).wait_send()

            @pl.when(row < r)
            def _():
                zcopy(h, row).wait_send()

        def drain_r(s, carry, h=h):
            for u in range(SUBS):
                rcopy(h, u, s).wait_send()
            return carry

        lax.fori_loop(0, n - 1, drain_r, 0)
    for cp in dq_cp + [kvg_cp, wg_cp]:
        cp.wait()


def hand_on(*refs):
    srcs, dsts, bufs, sems = refs[:3], refs[3:6], refs[6:9], refs[9]
    pieces = []
    for i in range(3):
        step = srcs[i].shape[0] // 2
        for k in range(2):
            rows = slice(k * step, (k + 1) * step)
            pieces.append((
                pltpu.make_async_copy(srcs[i].at[rows], bufs[i].at[rows], sems.at[0, i, k]),
                pltpu.make_async_copy(bufs[i].at[rows], dsts[i].at[rows], sems.at[1, i, k])))
    for load, _ in pieces:
        load.start()
    for load, store in pieces:
        load.wait()
        store.start()
    for _, store in pieces:
        store.wait()


def shards(queries, keys_values, log_sums, out_grad, inputs, chosen):
    tok = queries.shape[0]
    heads_here = queries.shape[1] // DH
    kv_heads = keys_values.shape[1] // (2 * DH)
    group = heads_here // kv_heads
    nqb, nblk = tok // QB, tok // BLK
    n = lax.axis_size("kv")
    rows_n = n // 2
    row_width = keys_values.shape[1]
    cap = nblk // 2
    pos_w = pl.cdiv(n * nblk, 128) * 128
    lanes = group * QB
    width = group * DH
    sub_w = width // SUBS
    drow = inputs.shape[1] // n
    vmem = pl.BlockSpec(memory_space=pltpu.VMEM)
    smem = pl.BlockSpec(memory_space=pltpu.SMEM)
    hbm = pl.BlockSpec(memory_space=pl.ANY)
    per_head = lambda shape, dtype: [pltpu.VMEM(shape, dtype)] * kv_heads
    bf, f32 = jnp.bfloat16, jnp.float32
    keys = NSEL * BLK
    dma = pltpu.SemaphoreType.DMA
    scratch = (
        per_head((rows_n * (nblk + cap), BLK, 2 * DH), bf)
        + per_head((nqb, width, QB), bf)
        + per_head((rows_n, nblk, BLK, 2 * DH), f32)
        + per_head((nblk, BLK, 2 * DH), bf) * rows_n
        + per_head((cap, BLK, 2 * DH), bf) * rows_n
        + per_head((rows_n, cap, BLK, 2 * DH), bf)
        + per_head((cap + 1, BLK, 2 * DH), bf) * rows_n
        + per_head((rows_n, nblk, BLK, 2 * DH), bf)
        + per_head((rows_n, nblk, BLK, 2 * DH), bf)
        + per_head((SUBS, n - 1, sub_w, drow), bf)
        + per_head((SUBS, n - 1, sub_w, drow), bf)
        + [
            pltpu.VMEM((n, tok, drow), bf),
            pltpu.VMEM((2 * DH, 2 * lanes), bf),
            pltpu.VMEM((keys, 2 * DH), bf),
            pltpu.VMEM((keys, lanes), f32),
            pltpu.VMEM((keys, lanes), f32),
            pltpu.VMEM((keys, 2 * lanes), bf),
            pltpu.VMEM((nqb * NSEL + 1, BLK, 2 * DH), f32),
            pltpu.VMEM((tok, heads_here * DH), bf),
            pltpu.VMEM((tok, heads_here * DH), bf),
            pltpu.VMEM((nqb, heads_here, QB), f32),
            pltpu.VMEM((tok, heads_here * DH), bf),
            pltpu.VMEM((tok, row_width), f32),
            pltpu.VMEM((drow, heads_here * DH), f32),
            pltpu.VMEM((8, 128), jnp.int32),
            pltpu.VMEM((8, pos_w), jnp.int32),
            pltpu.VMEM((2 * n, 128), jnp.int32),
            pltpu.VMEM((nqb, NSEL), jnp.int32),
            pltpu.VMEM((8, 128), jnp.int32),
            pltpu.SMEM((8, 128), jnp.int32),
            pltpu.SMEM((8, pos_w), jnp.int32),
            pltpu.SMEM((2 * n, 128), jnp.int32),
            pltpu.SMEM((8, 128), jnp.int32),
            dma((n,)),
            dma((kv_heads,)),
            dma((2,)),
            dma((3,)),
            dma((kv_heads + 2,)),
            dma((2,)),
            dma((kv_heads, rows_n)),
            dma((kv_heads, PIECES, rows_n)),
            dma((kv_heads, rows_n)),
            dma((kv_heads, rows_n)),
            dma((kv_heads, PIECES, rows_n)),
            dma((kv_heads, rows_n)),
            dma((kv_heads, rows_n)),
            dma((kv_heads, rows_n)),
            dma((kv_heads, rows_n)),
            dma((kv_heads, SUBS, n - 1)),
            dma((kv_heads, SUBS, n - 1)),
        ]
    )
    shapes = [
        jax.ShapeDtypeStruct((tok, heads_here * DH), bf),
        jax.ShapeDtypeStruct((tok, row_width), f32),
        jax.ShapeDtypeStruct((drow, heads_here * DH), f32),
    ]
    raw = pl.pallas_call(
        functools.partial(whole, n, kv_heads, group, tok),
        in_specs=[smem, vmem, vmem, hbm, hbm, hbm, hbm],
        out_specs=[hbm, hbm, hbm],
        out_shape=shapes,
        scratch_shapes=scratch,
        compiler_params=pltpu.CompilerParams(
            collective_id=0, has_side_effects=True, vmem_limit_bytes=63 * 1024 * 1024
        ),
    )(chosen, chosen, log_sums.T, queries, out_grad, keys_values.reshape(nblk, BLK, -1), inputs)
    return tuple(pl.pallas_call(
        hand_on,
        in_specs=[hbm] * 3,
        out_specs=[hbm] * 3,
        out_shape=shapes,
        scratch_shapes=[pltpu.VMEM(x.shape, x.dtype) for x in shapes] + [dma((2, 3, 2))],
    )(*raw))


def solution(mesh):
    in_specs = (
        P("kv", "tp"),
        P("kv", "tp"),
        P("kv", "tp"),
        P("kv", "tp"),
        P("kv", None),
        P("kv", None),
    )
    out_specs = (P("kv", "tp"), P("kv", "tp"), P("kv", "tp"))
    return jax.shard_map(shards, mesh=mesh, in_specs=in_specs, out_specs=out_specs, check_vma=False)
```

time: 141 us -> 122 us (0.87)
  Pallas kernels: 129 us -> 121 us
  local copies, waits for them, and re-layouts: 7.74 us -> 0 us
  other arithmetic: 2.67 us -> 0 us
    pallas_call x1, Pallas kernels: 129 us -> 119 us  [shards(): pl.pallas_call(functools.partial(whole, n, kv_heads, group, tok), in_spec...]
    unnamed x3 -> x0, local copies, waits for them, and re-layouts: 6.39 us -> none
    pallas_call x0 -> x1, Pallas kernels: none -> 2.59 us  [shards(): pl.pallas_call(hand_on, in_specs=[hbm] * 3, out_specs=[hbm] * 3, out_shap...]
where the time goes in v2:
time: 122 us
  Pallas kernels  121 us (99%)
    pallas_call x1, Pallas kernels, shards(): pl.pallas_call(functools.partial(whole, n, kv_heads, group, tok), in_spec...  119 us
    pallas_call x1, Pallas kernels, shards(): pl.pallas_call(hand_on, in_specs=[hbm] * 3, out_specs=[hbm] * 3, out_shap...  2.59 us

profile of v2, /device:TPU:0, one launch (start us, length us, event | category | flops | bytes accessed | tf_op | source)
XLA Modules:
  0.0 121.9 jit_solution(6266920393595928597)
XLA Ops:
  0.6 118.7 %shard_map.85 = (bf16[768,512]{1,0:T(8,128)(2,1)}, f32[768,256]{1,0:T(8,128)}, f32[512,512]{1,0:T(8,128)}) custom-call(s32[6,16]{1,0:T(8,128)} %list_ref.1, s32[6,16]{1,0:T(8,128)} %list_ref.1, f32[8,768]{1,0:T(8,128)} %bitcast.3, bf16[768,512]{1,0:T(8,128)(2,1)} %q_hbm.1, bf16[768,512]{1,0:T(8,128)(2,1)} %do_hbm.1, bf16[12,64,256]{2,1,0:T(8,128)(2,1)} %bitcast.2, ...), custom_call_target="tpu_custom_call" | custom-call | tf_op jit(solution)/shard_map/pallas_call | solution.py:585
  119.3 2.6 %shard_map.86 = (bf16[768,512]{1,0:T(8,128)(2,1)}, f32[768,256]{1,0:T(8,128)}, f32[512,512]{1,0:T(8,128)}) custom-call(bf16[768,512]{1,0:T(8,128)(2,1)} %get-tuple-element.6.refs_0_, f32[768,256]{1,0:T(8,128)} %get-tuple-element.7.refs_1_, f32[512,512]{1,0:T(8,128)} %get-tuple-element.8.refs_2_), custom_call_target="tpu_custom_call" | custom-call | tf_op jit(solution)/shard_map/pallas_call | solution.py:595

commit v3 on v2

--- a/solution.py
+++ b/solution.py
@@ -16,9 +16,10 @@
 MESH = pl.DeviceIdType.MESH
 SUBS = 4
 PIECES = 2
-
-
-def whole(n, kv_heads, group, tok, chosen_ref, list_ref, ls_ref, q_hbm, do_hbm, kv_hbm, inp_hbm,
+OFFS = (1, 3)
+
+
+def whole(n, kv_heads, group, tok, chosen_hbm, ls_hbm, q_hbm, do_hbm, kv_hbm, inp_hbm,
           dq_hbm, kvg_hbm, wg_hbm, *scratch):
     it = iter(scratch)
     tabs = [next(it) for _ in range(kv_heads)]
@@ -35,7 +36,7 @@
     rrecv = [next(it) for _ in range(kv_heads)]
     inp, w1, kv_scr, p_scr, dp_scr, a_scr, both_scr = [next(it) for _ in range(7)]
     q_ref, do_ref, ls_t, dq_ref, kvg_ref, wg_ref, table_v, pos_v, req_v, plist_v, pch_v = [next(it) for _ in range(11)]
-    table, pos_ref, req_ref, pch_ref = [next(it) for _ in range(4)]
+    table, pos_ref, req_ref, pch_ref, chosen_ref, list_ref, ls_ref = [next(it) for _ in range(7)]
     (inp_sem, own_sem, in_sem, tab_sem, out_sem, list_sem, loc_sem, fz_s, fy_s, fy_r, f_r, gy_s, gy_r, gz_s, gz_r, r_s, r_r) = [next(it) for _ in range(17)]
 
     nqb = tok // QB
@@ -59,37 +60,41 @@
     pos_me = jnp.where(c == 0, r, n - 1 - r)
     ring_to = (at_pos(pos_me + 1), at_pos(pos_me - 1))
 
-    barrier = pltpu.get_barrier_semaphore()
-    pl.semaphore_signal(barrier, inc=1, device_id={"kv": partner}, device_id_type=MESH)
-
-    @pl.when(has_up)
-    def _():
-        pl.semaphore_signal(barrier, inc=1, device_id={"kv": up}, device_id_type=MESH)
-
-    @pl.when(has_down)
-    def _():
-        pl.semaphore_signal(barrier, inc=1, device_id={"kv": down}, device_id_type=MESH)
-
     own_cp = [
         pltpu.make_async_copy(kv_hbm.at[:, :, h * 2 * DH:(h + 1) * 2 * DH], arr[h][0], own_sem.at[h])
         for h in range(kv_heads)
     ]
-    for cp in own_cp:
+    small_cp = [
+        pltpu.make_async_copy(chosen_hbm, list_ref, in_sem.at[2]),
+        pltpu.make_async_copy(chosen_hbm, chosen_ref, in_sem.at[3]),
+        pltpu.make_async_copy(ls_hbm, ls_ref, in_sem.at[4]),
+    ]
+    for cp in own_cp[:1] + small_cp + own_cp[1:]:
         cp.start()
+    barrier = pltpu.get_barrier_semaphore()
+    pl.semaphore_signal(barrier, inc=1, device_id={"kv": partner}, device_id_type=MESH)
+
+    @pl.when(has_up)
+    def _():
+        pl.semaphore_signal(barrier, inc=1, device_id={"kv": up}, device_id_type=MESH)
+
+    @pl.when(has_down)
+    def _():
+        pl.semaphore_signal(barrier, inc=1, device_id={"kv": down}, device_id_type=MESH)
+
     drow = inp_hbm.shape[1] // n
     inp_cp = [
         pltpu.make_async_copy(inp_hbm.at[:, i * drow:(i + 1) * drow], inp.at[i], inp_sem.at[i]) for i in range(n)
     ]
-    for cp in inp_cp:
-        cp.start()
     in_cp = [
         pltpu.make_async_copy(q_hbm, q_ref, in_sem.at[0]),
         pltpu.make_async_copy(do_hbm, do_ref, in_sem.at[1]),
     ]
     for cp in in_cp:
         cp.start()
-    for cp in own_cp:
-        cp.wait()
+    for cp in inp_cp:
+        cp.start()
+    own_cp[0].wait()
     pl.semaphore_wait(barrier, 1 + has_up.astype(jnp.int32) + has_down.astype(jnp.int32))
 
     piece_n = nblk // PIECES
@@ -262,6 +267,8 @@
                     kvg_ref[k * BLK:(k + 1) * BLK, cols] += (
                         yrecv[h][row][pos_ref[nqb + 1, (2 * row + c) * nblk + k]].astype(jnp.float32))
 
+        kvg_cp[h].start()
+
     def rcopy(h, u, s):
         return pltpu.make_async_remote_copy(
             src_ref=rsend[h].at[u, s], dst_ref=rrecv[h].at[u, s], send_sem=r_s.at[h, u, s],
@@ -291,16 +298,16 @@
                 rsend[h][u, s] = piece.astype(jnp.bfloat16)
                 rcopy(h, u, s).start()
 
-    def ring_end():
-        parts = [[partial_of(h, d, me) for d in range(2)] for h in range(kv_heads)]
-        for h in range(kv_heads):
-            for d in range(2):
-                got = []
-                for v in range(SUBS // 2):
-                    u = d * (SUBS // 2) + v
-                    rcopy(h, u, n - 2).wait_recv()
-                    got.append(parts[h][d][v * sub_w:(v + 1) * sub_w] + rrecv[h][u, n - 2].astype(jnp.float32))
-                wg_ref[:, h * width + d * half:h * width + (d + 1) * half] = jnp.concatenate(got, axis=0).T
+    def ring_end(h):
+        parts = [partial_of(h, d, me) for d in range(2)]
+        for d in range(2):
+            got = []
+            for v in range(SUBS // 2):
+                u = d * (SUBS // 2) + v
+                rcopy(h, u, n - 2).wait_recv()
+                got.append(parts[d][v * sub_w:(v + 1) * sub_w] + rrecv[h][u, n - 2].astype(jnp.float32))
+            wg_ref[:, h * width + d * half:h * width + (d + 1) * half] = jnp.concatenate(got, axis=0).T
+        wg_cp[h].start()
 
     def pass_slot(h, slot):
         for row in range(rows_n - 1):
@@ -312,7 +319,6 @@
     list_cp = pltpu.make_async_remote_copy(
         src_ref=list_ref, dst_ref=plist_v, send_sem=list_sem.at[0], recv_sem=list_sem.at[1],
         device_id={"kv": partner}, device_id_type=MESH)
-    list_cp.start()
 
     def ranks(ref, ids, within):
         need = ids == ref[0, 0]
@@ -335,9 +341,11 @@
         return out
 
     with jax.named_scope("fetch_first"):
-        for h in range(kv_heads):
-            for f in range(PIECES):
-                forward(h, 0, f)
+        for f in range(PIECES):
+            forward(0, 0, f)
+        for cp in small_cp:
+            cp.wait()
+        list_cp.start()
         ids = lax.broadcasted_iota(jnp.int32, (1, pos_v.shape[1]), 1)
         owner = jnp.zeros_like(ids)
         for o in range(1, n):
@@ -356,6 +364,8 @@
             for j in range(NSEL):
                 at = jnp.where(ids == chosen_ref[qb, j], qb * NSEL + j, at)
             pos_v[qb:qb + 1, :] = at
+        for f in range(PIECES):
+            forward(0, 1, f)
         list_cp.wait_recv()
         pch_v[:nqb, :NSEL] = plist_v[...]
         cp = pltpu.make_async_copy(pch_v, pch_ref, tab_sem.at[0])
@@ -373,20 +383,24 @@
             cp.start()
         for cp in tab_cp:
             cp.wait()
+        across(0, 0)
+        across(0, 1)
+        w1[...] = jnp.zeros_like(w1)
+        both_scr[nqb * NSEL] = jnp.zeros((BLK, 2 * DH), jnp.float32)
         for h in range(kv_heads):
-            across(h, 0)
-        for k in range(1, rows_n):
+            for row in range(rows_n):
+                yrecv[h][row][cap] = jnp.zeros((BLK, 2 * DH), jnp.bfloat16)
+        for qb in range(nqb):
+            ls_t[qb] = ls_ref[:, qb * QB:(qb + 1) * QB]
+        for k in range(2, rows_n):
             for f in range(PIECES):
                 forward(0, k, f)
             across(0, k)
-            if k == 1:
-                w1[...] = jnp.zeros_like(w1)
-                both_scr[nqb * NSEL] = jnp.zeros((BLK, 2 * DH), jnp.float32)
-                for h in range(kv_heads):
-                    for row in range(rows_n):
-                        yrecv[h][row][cap] = jnp.zeros((BLK, 2 * DH), jnp.bfloat16)
-                for qb in range(nqb):
-                    ls_t[qb] = ls_ref[:, qb * QB:(qb + 1) * QB]
+        for h in range(1, kv_heads):
+            own_cp[h].wait()
+            for f in range(PIECES):
+                forward(h, 0, f)
+            across(h, 0)
         arrived(0)
         for cp in in_cp:
             cp.wait()
@@ -412,7 +426,7 @@
                     def _():
                         with jax.named_scope(f"ring{h - 1}"):
                             ring(h - 1, k + 1, False)
-                        pass_slot(h - 1, k)
+                        pass_slot(h - 1, k + 1 - OFFS[h - 1])
             return carry
 
         lax.fori_loop(0, nqb, loop, 0)
@@ -430,26 +444,30 @@
             with jax.named_scope("arrive_next"):
                 arrived(h + 1)
 
+    kvg_cp = [pltpu.make_async_copy(
+        kvg_ref.at[:, h * 2 * DH:(h + 1) * 2 * DH], kvg_hbm.at[:, h * 2 * DH:(h + 1) * 2 * DH],
+        out_sem.at[kv_heads + h]) for h in range(kv_heads)]
+    wg_cp = [pltpu.make_async_copy(
+        wg_ref.at[:, h * width:(h + 1) * width], wg_hbm.at[:, h * width:(h + 1) * width],
+        out_sem.at[2 * kv_heads + h]) for h in range(kv_heads)]
+
     def ring_loop(s, carry):
         for h in range(kv_heads):
             @pl.when(s + early[h] <= n - 2)
             def _():
                 with jax.named_scope(f"ring{h}"):
                     ring(h, s + early[h], False)
-            pass_slot(h, s - 1 + early[h] if early[h] else s - 2)
+            pass_slot(h, s + early[h] - OFFS[h])
+            if early[h]:
+                @pl.when(s == n - 2)
+                def _():
+                    with jax.named_scope(f"keep{h}"):
+                        keep(h)
+                    with jax.named_scope(f"ring_end{h}"):
+                        ring_end(h)
         return carry
 
     lax.fori_loop(1, n - 1, ring_loop, 0)
-    for h in range(kv_heads):
-        with jax.named_scope(f"keep{h}"):
-            keep(h)
-    kvg_cp = pltpu.make_async_copy(kvg_ref, kvg_hbm, out_sem.at[kv_heads])
-    kvg_cp.start()
-    with jax.named_scope("ring_end"):
-        ring_end()
-    wg_cp = pltpu.make_async_copy(wg_ref, wg_hbm, out_sem.at[kv_heads + 1])
-    wg_cp.start()
-
     list_cp.wait_send()
     for h in range(kv_heads):
         for k in range(rows_n):
@@ -477,8 +495,17 @@
                 rcopy(h, u, s).wait_send()
             return carry
 
-        lax.fori_loop(0, n - 1, drain_r, 0)
-    for cp in dq_cp + [kvg_cp, wg_cp]:
+        lax.fori_loop(0, n - 2, drain_r, 0)
+    for h in range(kv_heads):
+        if not early[h]:
+            with jax.named_scope(f"keep{h}"):
+                keep(h)
+            with jax.named_scope(f"ring_end{h}"):
+                ring_end(h)
+    for h in range(kv_heads):
+        for u in range(SUBS):
+            rcopy(h, u, n - 2).wait_send()
+    for cp in dq_cp + kvg_cp + wg_cp:
         cp.wait()
 
 
@@ -516,8 +543,6 @@
     width = group * DH
     sub_w = width // SUBS
     drow = inputs.shape[1] // n
-    vmem = pl.BlockSpec(memory_space=pltpu.VMEM)
-    smem = pl.BlockSpec(memory_space=pltpu.SMEM)
     hbm = pl.BlockSpec(memory_space=pl.ANY)
     per_head = lambda shape, dtype: [pltpu.VMEM(shape, dtype)] * kv_heads
     bf, f32 = jnp.bfloat16, jnp.float32
@@ -558,11 +583,14 @@
             pltpu.SMEM((8, pos_w), jnp.int32),
             pltpu.SMEM((2 * n, 128), jnp.int32),
             pltpu.SMEM((8, 128), jnp.int32),
+            pltpu.SMEM((nqb, NSEL), jnp.int32),
+            pltpu.VMEM((nqb, NSEL), jnp.int32),
+            pltpu.VMEM((heads_here, tok), f32),
             dma((n,)),
             dma((kv_heads,)),
-            dma((2,)),
+            dma((5,)),
             dma((3,)),
-            dma((kv_heads + 2,)),
+            dma((3 * kv_heads,)),
             dma((2,)),
             dma((kv_heads, rows_n)),
             dma((kv_heads, PIECES, rows_n)),
@@ -584,14 +612,14 @@
     ]
     raw = pl.pallas_call(
         functools.partial(whole, n, kv_heads, group, tok),
-        in_specs=[smem, vmem, vmem, hbm, hbm, hbm, hbm],
+        in_specs=[hbm] * 6,
         out_specs=[hbm, hbm, hbm],
         out_shape=shapes,
         scratch_shapes=scratch,
         compiler_params=pltpu.CompilerParams(
             collective_id=0, has_side_effects=True, vmem_limit_bytes=63 * 1024 * 1024
         ),
-    )(chosen, chosen, log_sums.T, queries, out_grad, keys_values.reshape(nblk, BLK, -1), inputs)
+    )(chosen, log_sums.T, queries, out_grad, keys_values.reshape(nblk, BLK, -1), inputs)
     return tuple(pl.pallas_call(
         hand_on,
         in_specs=[hbm] * 3,

time: 122 us -> 113 us (0.926)
  Pallas kernels: 121 us -> 113 us
    pallas_call x1, Pallas kernels: 119 us -> 110 us  [shards(): pl.pallas_call(functools.partial(whole, n, kv_heads, group, tok), in_spec...]
where the time goes in v3:
time: 113 us
  Pallas kernels  113 us (100%)
    pallas_call x1, Pallas kernels, shards(): pl.pallas_call(functools.partial(whole, n, kv_heads, group, tok), in_spec...  110 us
    pallas_call x1, Pallas kernels, shards(): pl.pallas_call(hand_on, in_specs=[hbm] * 3, out_specs=[hbm] * 3, out_shap...  2.59 us

profile of v3, /device:TPU:0, one launch (start us, length us, event | category | flops | bytes accessed | tf_op | source)
XLA Modules:
  0.0 113.3 jit_solution(13366904773920478239)
XLA Ops:
  0.6 110.0 %shard_map.85 = (bf16[768,512]{1,0:T(8,128)(2,1)}, f32[768,256]{1,0:T(8,128)}, f32[512,512]{1,0:T(8,128)}) custom-call(s32[6,16]{1,0:T(8,128)} %chosen_hbm.1, f32[8,768]{1,0:T(8,128)} %bitcast.3, bf16[768,512]{1,0:T(8,128)(2,1)} %q_hbm.1, bf16[768,512]{1,0:T(8,128)(2,1)} %do_hbm.1, bf16[12,64,256]{2,1,0:T(8,128)(2,1)} %bitcast.2, bf16[768,4096]{1,0:T(8,128)(2,1)} %inp_hbm.1), custom_call_target="tpu_custom_call" | custom-call | tf_op jit(solution)/shard_map/pallas_call | solution.py:613
  110.7 2.6 %shard_map.86 = (bf16[768,512]{1,0:T(8,128)(2,1)}, f32[768,256]{1,0:T(8,128)}, f32[512,512]{1,0:T(8,128)}) custom-call(bf16[768,512]{1,0:T(8,128)(2,1)} %get-tuple-element.6.refs_0_, f32[768,256]{1,0:T(8,128)} %get-tuple-element.7.refs_1_, f32[512,512]{1,0:T(8,128)} %get-tuple-element.8.refs_2_), custom_call_target="tpu_custom_call" | custom-call | tf_op jit(solution)/shard_map/pallas_call | solution.py:623

commit v4 on v3

--- a/solution.py
+++ b/solution.py
@@ -16,7 +16,8 @@
 MESH = pl.DeviceIdType.MESH
 SUBS = 4
 PIECES = 2
-OFFS = (1, 3)
+PASS_EARLY = (1, 3)
+PASS_LAST = (3, 1)
 
 
 def whole(n, kv_heads, group, tok, chosen_hbm, ls_hbm, q_hbm, do_hbm, kv_hbm, inp_hbm,
@@ -200,10 +201,11 @@
             src_ref=ysend[h].at[row], dst_ref=yrecv[h][row].at[:cap], send_sem=gy_s.at[h, row],
             recv_sem=gy_r.at[h, row], device_id={"kv": partner}, device_id_type=MESH)
 
-    def zcopy(h, row):
+    def zcopy(h, row, f):
+        part = pl.ds(f * piece_n, piece_n)
         return pltpu.make_async_remote_copy(
-            src_ref=zsend[h].at[row], dst_ref=zrecv[h].at[row], send_sem=gz_s.at[h, row],
-            recv_sem=gz_r.at[h, row], device_id={"kv": down}, device_id_type=MESH)
+            src_ref=zsend[h].at[row, part], dst_ref=zrecv[h].at[row, part], send_sem=gz_s.at[h, f, row],
+            recv_sem=gz_r.at[h, f, row], device_id={"kv": down}, device_id_type=MESH)
 
     def give(h):
         for row in range(rows_n):
@@ -227,32 +229,34 @@
     def pass_down(h, row):
         gsend(h, row).wait_recv()
 
+        def one(k, carry):
+            total = owns[h][row, k] + yrecv[h][row][pos_ref[nqb + 1, (2 * row + c) * nblk + k]].astype(jnp.float32)
+
+            @pl.when(has_up)
+            def _():
+                zsend[h][row, k] = (total + zrecv[h][row, k].astype(jnp.float32)).astype(jnp.bfloat16)
+
+            @pl.when(jnp.logical_not(has_up))
+            def _():
+                zsend[h][row, k] = total.astype(jnp.bfloat16)
+
+            return carry
+
+        for f in range(PIECES):
+            @pl.when(has_up)
+            def _():
+                zcopy(h, row, f).wait_recv()
+
+            lax.fori_loop(f * piece_n, (f + 1) * piece_n, one, 0)
+            zcopy(h, row, f).start()
+
+    def keep(h):
+        cols = slice(h * 2 * DH, (h + 1) * 2 * DH)
+
         @pl.when(has_up)
         def _():
-            zcopy(h, row).wait_recv()
-
-        def one(k, carry):
-            total = owns[h][row, k] + yrecv[h][row][pos_ref[nqb + 1, (2 * row + c) * nblk + k]].astype(jnp.float32)
-
-            @pl.when(has_up)
-            def _():
-                zsend[h][row, k] = (total + zrecv[h][row, k].astype(jnp.float32)).astype(jnp.bfloat16)
-
-            @pl.when(jnp.logical_not(has_up))
-            def _():
-                zsend[h][row, k] = total.astype(jnp.bfloat16)
-
-            return carry
-
-        lax.fori_loop(0, nblk, one, 0)
-        zcopy(h, row).start()
-
-    def keep(h):
-        cols = slice(h * 2 * DH, (h + 1) * 2 * DH)
-
-        @pl.when(has_up)
-        def _():
-            zcopy(h, r).wait_recv()
+            for f in range(PIECES):
+                zcopy(h, r, f).wait_recv()
             kvg_ref[:, cols] = (owns[h][r] + zrecv[h][r].astype(jnp.float32)).reshape(tok, 2 * DH)
 
         @pl.when(jnp.logical_not(has_up))
@@ -286,10 +290,10 @@
         return total
 
     def ring(h, s, first):
-        for d in range(2):
-            target = at_pos(pos_me - 1 - s) if d == 0 else at_pos(pos_me + 1 + s)
-            part = partial_of(h, d, target)
-            for v in range(SUBS // 2):
+        parts = [partial_of(h, d, at_pos(pos_me - 1 - s) if d == 0 else at_pos(pos_me + 1 + s)) for d in range(2)]
+        for v in range(SUBS // 2):
+            for d in range(2):
+                part = parts[d]
                 u = d * (SUBS // 2) + v
                 piece = part[v * sub_w:(v + 1) * sub_w]
                 if not first:
@@ -309,9 +313,11 @@
             wg_ref[:, h * width + d * half:h * width + (d + 1) * half] = jnp.concatenate(got, axis=0).T
         wg_cp[h].start()
 
-    def pass_slot(h, slot):
+    def pass_slot(h, step):
+        offset, skew = PASS_EARLY if early[h] else PASS_LAST
+        skew = min(skew, (n - 2 + early[h] - offset) // max(rows_n - 2, 1))
         for row in range(rows_n - 1):
-            @pl.when((slot - (rows_n - 1 - r) == row) & (row < r))
+            @pl.when((step == offset + row + skew * (rows_n - 1 - r)) & (row < r))
             def _():
                 with jax.named_scope(f"pass{h}"):
                     pass_down(h, row)
@@ -426,7 +432,7 @@
                     def _():
                         with jax.named_scope(f"ring{h - 1}"):
                             ring(h - 1, k + 1, False)
-                        pass_slot(h - 1, k + 1 - OFFS[h - 1])
+                        pass_slot(h - 1, k + 1)
             return carry
 
         lax.fori_loop(0, nqb, loop, 0)
@@ -457,7 +463,7 @@
             def _():
                 with jax.named_scope(f"ring{h}"):
                     ring(h, s + early[h], False)
-            pass_slot(h, s + early[h] - OFFS[h])
+            pass_slot(h, s + early[h])
             if early[h]:
                 @pl.when(s == n - 2)
                 def _():
@@ -488,7 +494,8 @@
 
             @pl.when(row < r)
             def _():
-                zcopy(h, row).wait_send()
+                for f in range(PIECES):
+                    zcopy(h, row, f).wait_send()
 
         def drain_r(s, carry, h=h):
             for u in range(SUBS):
@@ -498,10 +505,10 @@
         lax.fori_loop(0, n - 2, drain_r, 0)
     for h in range(kv_heads):
         if not early[h]:
+            with jax.named_scope(f"ring_end{h}"):
+                ring_end(h)
             with jax.named_scope(f"keep{h}"):
                 keep(h)
-            with jax.named_scope(f"ring_end{h}"):
-                ring_end(h)
     for h in range(kv_heads):
         for u in range(SUBS):
             rcopy(h, u, n - 2).wait_send()
@@ -599,8 +606,8 @@
             dma((kv_heads, PIECES, rows_n)),
             dma((kv_heads, rows_n)),
             dma((kv_heads, rows_n)),
-            dma((kv_heads, rows_n)),
-            dma((kv_heads, rows_n)),
+            dma((kv_heads, PIECES, rows_n)),
+            dma((kv_heads, PIECES, rows_n)),
             dma((kv_heads, SUBS, n - 1)),
             dma((kv_heads, SUBS, n - 1)),
         ]

time: 113 us -> 112 us (level)
  Pallas kernels: 113 us -> 111 us
    pallas_call x1, Pallas kernels: 110 us -> 108 us  [shards(): pl.pallas_call(functools.partial(whole, n, kv_heads, group, tok), in_spec...]
where the time goes in v4:
time: 112 us
  Pallas kernels  111 us (99%)
    pallas_call x1, Pallas kernels, shards(): pl.pallas_call(functools.partial(whole, n, kv_heads, group, tok), in_spec...  108 us
    pallas_call x1, Pallas kernels, shards(): pl.pallas_call(hand_on, in_specs=[hbm] * 3, out_specs=[hbm] * 3, out_shap...  2.59 us

profile of v4, /device:TPU:0, one launch (start us, length us, event | category | flops | bytes accessed | tf_op | source)
XLA Modules:
  0.0 111.6 jit_solution(801571753887041011)
XLA Ops:
  0.6 108.4 %shard_map.85 = (bf16[768,512]{1,0:T(8,128)(2,1)}, f32[768,256]{1,0:T(8,128)}, f32[512,512]{1,0:T(8,128)}) custom-call(s32[6,16]{1,0:T(8,128)} %chosen_hbm.1, f32[8,768]{1,0:T(8,128)} %bitcast.3, bf16[768,512]{1,0:T(8,128)(2,1)} %q_hbm.1, bf16[768,512]{1,0:T(8,128)(2,1)} %do_hbm.1, bf16[12,64,256]{2,1,0:T(8,128)(2,1)} %bitcast.2, bf16[768,4096]{1,0:T(8,128)(2,1)} %inp_hbm.1), custom_call_target="tpu_custom_call" | custom-call | tf_op jit(solution)/shard_map/pallas_call | solution.py:620
  109.0 2.6 %shard_map.86 = (bf16[768,512]{1,0:T(8,128)(2,1)}, f32[768,256]{1,0:T(8,128)}, f32[512,512]{1,0:T(8,128)}) custom-call(bf16[768,512]{1,0:T(8,128)(2,1)} %get-tuple-element.6.refs_0_, f32[768,256]{1,0:T(8,128)} %get-tuple-element.7.refs_1_, f32[512,512]{1,0:T(8,128)} %get-tuple-element.8.refs_2_), custom_call_target="tpu_custom_call" | custom-call | tf_op jit(solution)/shard_map/pallas_call | solution.py:630
